TPU v7x, 512 devices: a whole 4x4x16 slice. The times are simulated.
512 devices in a mesh: kv: 64 (over z, y), tp: 8 (over x, core).
Axes of the slice: x: 4, y: 4, z: 16, core: 2. Of those that a mesh axis runs over, the one named last changes fastest.
Arguments:
- stream: bfloat16 [32, 4096], P(None, 'kv'), may hold values from -32 to 32
- gain_in: bfloat16 [4096], P('kv'), may hold values from 0.099609375 to 1.8984375
- w_query: bfloat16 [4096, 2048], P('kv', 'tp'), may hold values from -0.09375 to 0.09375
- w_key: bfloat16 [4096, 2048], P('kv', 'tp'), may hold values from -0.09375 to 0.09375
- w_value: bfloat16 [4096, 2048], P('kv', 'tp'), may hold values from -0.09375 to 0.09375
- w_forget: bfloat16 [4096, 16], replicated, may hold values from -0.09375 to 0.09375
- keys_cache: bfloat16 [32, 16, 8192, 128], P(None, 'tp', 'kv'), may hold values from -136 to 136
- values_cache: bfloat16 [32, 16, 8192, 128], P(None, 'tp', 'kv'), may hold values from -6 to 6
- decay_cache: float32 [32, 16, 8192], P(None, 'tp', 'kv'), may hold values from -1283 to 0
- lengths: int32 [32], replicated, may hold values from 1 to 8192, 104889 in all
- gain_att: bfloat16 [2048], P('tp'), may hold values from 0.099609375 to 1.8984375
- w_out: bfloat16 [2048, 4096], P('tp', 'kv'), may hold values from -0.125 to 0.125
- gain_mlp: bfloat16 [4096], P('kv'), may hold values from 0.099609375 to 1.8984375
- w_up: bfloat16 [4096, 16384], P('kv', 'tp'), may hold values from -0.09375 to 0.09375
- w_down: bfloat16 [16384, 4096], P('tp', 'kv'), may hold values from -0.046875 to 0.046875
Outputs:
- updated: bfloat16 [32, 4096], P(None, 'kv')
Inputs may be any that keep to these rules, and one draw needn't show every extreme that they name: `lengths`: one sequence has all 8192 positions live.
All inputs are finite; a program needn't handle non-finite values.
Results may differ from a plain program's by a relative error of at most 0.012.
The roundings to bfloat16 on the way count: a program that leaves them out, or rounds other values in their place, can miss the bound.
Values may be sent and summed in bfloat16 or wider, within the bound.
No kernel may reach another device: no remote copies, remote signals or barrier semaphores. Data moves between devices by JAX's collectives and lax.ppermute only.
A program may use at most 64 MiB of HBM per device.

v0:
```python
import math

import jax
import jax.numpy as jnp
from jax import lax
from jax.sharding import Mesh
from jax.sharding import PartitionSpec as P

KV = ("kv_0", "kv_1")


norm_eps = 1e-06
masked_score = -1e30


def padded_to(lines, devices):
    spare = -lines.shape[0] % devices
    if not spare:
        return lines
    return jnp.concatenate([lines, jnp.zeros((spare, *lines.shape[1:]), lines.dtype)])


def laid_out(parts, dim):
    parts = jnp.moveaxis(parts, 0, dim)
    lengths = parts.shape
    return parts.reshape(*lengths[:dim], lengths[dim] * lengths[dim + 1], *lengths[dim + 2 :])


def sent_to_all(value, axis):
    copies = jnp.broadcast_to(value, (lax.axis_size(axis), *value.shape))
    return lax.all_to_all(copies, axis, split_axis=0, concat_axis=0, tiled=True)


def gather_directly(value, axis, dim):
    return laid_out(sent_to_all(value, axis), dim)


def cut_along(value, dim, devices):
    lengths = value.shape
    parts = value.reshape(*lengths[:dim], devices, lengths[dim] // devices, *lengths[dim + 1 :])
    return jnp.moveaxis(parts, dim, 0)


def sum_at_owner(value, axis, dim):
    devices = lax.axis_size(axis)
    parts = lax.all_to_all(cut_along(value, dim, devices), axis, 0, 0, tiled=True)
    return jnp.sum(parts, axis=0)


def sum_by_parts(value, axes):
    padded = padded_to(value, lax.axis_size(axes))
    whole = gather_directly(sum_at_owner(padded, axes, 0), axes, 0)
    return lax.slice_in_dim(whole, 0, len(value)).reshape(value.shape)


def together(arrays, axis):
    line, at, finished = (jnp.concatenate([a.reshape(-1) for a in arrays]), 0, [])
    so_far = sum_by_parts(line, axis)
    for a in arrays:
        finished.append(so_far[at : at + a.size].reshape(a.shape))
        at += a.size
    return tuple(finished)


def all_in_one(value, axis):
    leaves = jax.tree.leaves(value)
    turns = sorted(range(len(leaves)), key=lambda k: -leaves[k].size)
    width = (1, *leaves[turns[0]].shape)[-1]
    lines = [
        jnp.pad(leaves[k].reshape(-1), (0, -leaves[k].size % width)).reshape(-1, width)
        for k in turns
    ]
    both, at, found = (lax.all_gather(jnp.concatenate(lines), axis), 0, {})
    for k, line in zip(turns, lines):
        share = both[:, at : at + len(line)].reshape(len(both), -1)
        found[k] = share[:, : leaves[k].size].reshape(-1, *leaves[k].shape)
        at += len(line)
    numbers = iter(range(len(leaves)))
    return jax.tree.map(lambda _: found[next(numbers)], value)


def joined_all(value, axes, combine):
    for axis in axes:
        pieces = all_in_one(value, axis)
        value = jax.tree.map(lambda part: part[0], pieces)
        for k in range(1, lax.axis_size(axis)):
            value = combine(value, jax.tree.map(lambda part: part[k], pieces))
    return value


def over_copies(value, axis):
    everything = sent_to_all(value, axis)
    return jnp.sum(everything, axis=0)


def fold_parts(left_part, right_part):
    peak_all = jnp.maximum(left_part[0], right_part[0])
    weight_one = jnp.exp(left_part[0] - peak_all)
    weight_two = jnp.exp(right_part[0] - peak_all)
    total_sum = left_part[1] * weight_one + right_part[1] * weight_two
    merged = left_part[2] * weight_one[..., None] + right_part[2] * weight_two[..., None]
    return (peak_all, total_sum, merged)


def per_device(
    stream,
    gain_in,
    w_query,
    w_key,
    w_value,
    w_forget,
    keys_cache,
    values_cache,
    decay_cache,
    lengths,
    gain_att,
    w_out,
    gain_mlp,
    w_up,
    w_down,
):
    kv_index = lax.axis_index(KV)
    tp_index = lax.axis_index("tp")
    kv_count = lax.axis_size(KV)
    seqs_here, cols_here = stream.shape
    heads_here = keys_cache.shape[1]
    pos_here = keys_cache.shape[2]
    head_dim = keys_cache.shape[3]
    width_all = cols_here * kv_count
    score_scale = 1.0 / math.sqrt(head_dim)
    stream_float = stream.astype(jnp.float32)
    scaled = (stream_float * gain_in.astype(jnp.float32)).astype(jnp.bfloat16)
    square_sum = jnp.sum(stream_float * stream_float, axis=1)
    forget_rows = lax.dynamic_slice(
        w_forget, (kv_index * cols_here, tp_index * heads_here), (cols_here, heads_here)
    )
    part_query = jnp.dot(scaled, w_query, preferred_element_type=jnp.float32)
    part_key = jnp.dot(scaled, w_key, preferred_element_type=jnp.float32)
    part_value = jnp.dot(scaled, w_value, preferred_element_type=jnp.float32)
    part_forget = jnp.dot(scaled, forget_rows, preferred_element_type=jnp.float32)
    part_query, part_key, part_value, part_forget, square_total = together(
        (part_query, part_key, part_value, part_forget, square_sum), KV
    )
    scale_in = lax.rsqrt(square_total / width_all + norm_eps)[:, None]
    queries = (part_query * scale_in).astype(jnp.bfloat16).reshape(seqs_here, heads_here, head_dim)
    key_new = (part_key * scale_in).astype(jnp.bfloat16).reshape(seqs_here, heads_here, head_dim)
    value_new = (
        (part_value * scale_in).astype(jnp.bfloat16).reshape(seqs_here, heads_here, head_dim)
    )
    forget = jax.nn.log_sigmoid(part_forget * scale_in)
    attention_logits = (
        jnp.einsum("shd,shpd->shp", queries, keys_cache, preferred_element_type=jnp.float32)
        * score_scale
    )
    attention_logits = attention_logits + forget[:, :, None] + decay_cache
    cache_positions = kv_index * pos_here + lax.iota(jnp.int32, pos_here)
    live_mask = (cache_positions[None, :] < lengths[:, None])[:, None, :]
    attention_logits = jnp.where(live_mask, attention_logits, masked_score)
    block_peak = jnp.max(attention_logits, axis=2)
    weights = jnp.where(live_mask, jnp.exp(attention_logits - block_peak[..., None]), 0.0)
    block_total = jnp.sum(weights, axis=2)
    block_out = jnp.einsum(
        "shp,shpd->shd",
        weights.astype(jnp.bfloat16),
        values_cache,
        preferred_element_type=jnp.float32,
    )
    peak_all, total_all, out_all = joined_all((block_peak, block_total, block_out), KV, fold_parts)
    own_score = (
        jnp.sum(queries.astype(jnp.float32) * key_new.astype(jnp.float32), axis=2) * score_scale
    )
    top_score = jnp.maximum(peak_all, own_score)
    past_weight = jnp.exp(peak_all - top_score)
    own_weight = jnp.exp(own_score - top_score)
    numerator = (
        out_all * past_weight[..., None] + value_new.astype(jnp.float32) * own_weight[..., None]
    )
    denominator = total_all * past_weight + own_weight
    attended = (numerator / denominator[..., None]).reshape(seqs_here, heads_here * head_dim)
    attended_in = (attended * gain_att.astype(jnp.float32)).astype(jnp.bfloat16)
    part_out = jnp.dot(attended_in, w_out, preferred_element_type=jnp.float32)
    att_squares = jnp.sum(attended * attended, axis=1)
    part_out, att_total = (over_copies(part_out, "tp"), over_copies(att_squares, "tp"))
    scale_att = lax.rsqrt(att_total / (attended.shape[1] * lax.axis_size("tp")) + norm_eps)[:, None]
    residual = (stream_float + scale_att * part_out).astype(jnp.bfloat16)
    residual_float = residual.astype(jnp.float32)
    mixer_in = (residual_float * gain_mlp.astype(jnp.float32)).astype(jnp.bfloat16)
    mixer_squares = jnp.sum(residual_float * residual_float, axis=1)
    part_up = jnp.dot(mixer_in, w_up, preferred_element_type=jnp.float32)
    square_cols = jnp.broadcast_to(mixer_squares[:, None], (seqs_here, kv_count))
    share_units, share_total = (sum_at_owner(part_up, KV, 1), sum_at_owner(square_cols, KV, 1))
    scale_mixer = lax.rsqrt(share_total / width_all + norm_eps)
    hidden_share = jnp.square(jax.nn.relu(share_units * scale_mixer)).astype(jnp.bfloat16)
    hidden = gather_directly(hidden_share, KV, 1)
    part_down = jnp.dot(hidden, w_down, preferred_element_type=jnp.float32)
    mixer_out = over_copies(part_down, "tp")
    return (residual_float + mixer_out).astype(jnp.bfloat16)


def solution(mesh):
    split = Mesh(mesh.devices.reshape(16, 4, mesh.shape["tp"]), ("kv_0", "kv_1", "tp"))
    return jax.shard_map(
        per_device,
        mesh=split,
        in_specs=(
            P(None, KV),
            P(KV),
            P(KV, "tp"),
            P(KV, "tp"),
            P(KV, "tp"),
            P(),
            P(None, "tp", KV, None),
            P(None, "tp", KV, None),
            P(None, "tp", KV),
            P(),
            P("tp"),
            P("tp", KV),
            P(KV),
            P(KV, "tp"),
            P("tp", KV),
        ),
        out_specs=P(None, KV),
        check_vma=False,
    )
```

profile of v0, /device:TPU:1, one launch (start us, length us, event | category | flops | bytes accessed | tf_op | source)
XLA Modules:
  0.0 224.7 jit_solution(15841474211591573087)
XLA Ops:
  0.0 0.8 convert_element_type.75
  0.8 0.8 fusion.60
  1.6 0.9 fusion.72
  2.6 0.9 convolution_bitcast_fusion.2
  3.5 0.9 convolution_bitcast_fusion.1
  4.5 0.9 convolution_bitcast_fusion
  5.8 34.1 %all_to_all.46 = f32[64,1,386]{2,1,0:T(1,128)S(1)} all-to-all(f32[64,1,386]{2,1,0:T(1,128)S(1)} %all_to_all.29), channel_id=1, replica_groups=mesh['kv_0'=16,'kv_1'=4,'tp'=8] {'kv_0','kv_1'}, dimensions={0} | all-to-all | bytes 197632 | tf_op jit(solution)/shard_map/all_to_all | solution.py:46
  40.7 6.3 %all-to-all-start.1 = ((f32[64,1,386]{2,1,0:T(1,128)}), f32[64,1,386]{2,1,0:T(1,128)S(1)}, u32[]{:S(2)}, u32[]{:S(2)}) async-start(f32[64,1,386]{2,1,0:T(1,128)} %broadcast_in_dim.32), calls=%async_computation.1 | async-start | bytes 262144 | tf_op jit(solution)/shard_map/all_to_all | solution.py:31
  48.3 0.7 broadcast_compare_fusion
  49.0 13.0 %all-to-all-done.1 = f32[64,1,386]{2,1,0:T(1,128)S(1)} async-done(((f32[64,1,386]{2,1,0:T(1,128)}), f32[64,1,386]{2,1,0:T(1,128)S(1)}, u32[]{:S(2)}, u32[]{:S(2)}) %all-to-all-start.1) | async-done | bytes 98848 | tf_op jit(solution)/shard_map/all_to_all | solution.py:31
  62.7 3.5 %slice.349 = f32[12352,2]{1,0:T(8,128)} reshape(f32[64,386]{1,0:T(8,128)S(1)} %reduce.6) | data formatting | bytes 197632 | tf_op jit(solution)/shard_map/slice | solution.py:60
  66.4 0.8 fusion.65
  67.4 1.2 fusion.56
  69.2 2.2 fusion.54
  71.5 22.8 %all-gather.2 = f32[16,66,128]{2,1,0:T(8,128)S(1)} all-gather(f32[1,66,128]{2,1,0:T(8,128)S(1)} %maximum_bitcast_fusion), channel_id=2, replica_groups=mesh['kv_0'=16,'kv_1'=4,'tp'=8] {'kv_0'}, dimensions={0}, use_global_device_ids=true | all-gather | bytes 574464 | tf_op jit(solution)/shard_map/all_gather | solution.py:73
  94.8 9.4 %all-gather.3 = f32[4,66,128]{2,1,0:T(8,128)S(1)} all-gather(f32[1,66,128]{2,1,0:T(8,128)S(1)} %maximum_bitcast_fusion.1), channel_id=3, replica_groups=mesh['kv_0'=16,'kv_1'=4,'tp'=8] {'kv_1'}, dimensions={0}, use_global_device_ids=true | all-gather | bytes 168960 | tf_op jit(solution)/shard_map/all_gather | solution.py:73
  108.3 17.4 %all-to-all-start.2 = ((f32[8,1,32]{2,1,0:T(1,128)}), f32[8,1,32]{2,1,0:T(1,128)S(1)}, u32[]{:S(2)}, u32[]{:S(2)}) async-start(f32[8,1,32]{2,1,0:T(1,128)} %broadcast_in_dim.35), calls=%async_computation.2 | async-start | bytes 8192 | tf_op jit(solution)/shard_map/all_to_all | solution.py:31
  126.8 0.7 reshape.1676
  127.6 2.6 %all-to-all-done.2 = f32[8,1,32]{2,1,0:T(1,128)S(1)} async-done(((f32[8,1,32]{2,1,0:T(1,128)}), f32[8,1,32]{2,1,0:T(1,128)S(1)}, u32[]{:S(2)}, u32[]{:S(2)}) %all-to-all-start.2) | async-done | bytes 1056 | tf_op jit(solution)/shard_map/all_to_all | solution.py:31
  130.2 3.9 %all-to-all-start.3 = ((f32[8,1,2048]{2,1,0:T(1,128)}), f32[8,1,2048]{2,1,0:T(1,128)S(1)}, u32[]{:S(2)}, u32[]{:S(2)}) async-start(f32[8,1,2048]{2,1,0:T(1,128)} %reshape.1676), calls=%async_computation.3 | async-start | bytes 131072 | tf_op jit(solution)/shard_map/all_to_all | solution.py:31
  134.2 4.8 %all-to-all-done.3 = f32[8,1,2048]{2,1,0:T(1,128)S(1)} async-done(((f32[8,1,2048]{2,1,0:T(1,128)}), f32[8,1,2048]{2,1,0:T(1,128)S(1)}, u32[]{:S(2)}, u32[]{:S(2)}) %all-to-all-start.3) | async-done | bytes 65568 | tf_op jit(solution)/shard_map/all_to_all | solution.py:31
  139.5 0.8 reduce.41
  141.3 6.8 %all-to-all-start.5 = ((f32[64,32,1]{1,2,0:T(1,128)}), f32[64,32,1]{1,2,0:T(1,128)S(1)}, u32[]{:S(2)}, u32[]{:S(2)}) async-start(f32[64,32,1]{1,2,0:T(1,128)} %transpose.61), calls=%async_computation.5 | async-start | bytes 65536 | tf_op jit(solution)/shard_map/all_to_all | solution.py:46
  148.6 1.6 copy.98
  150.2 2.4 %reshape.1678 = f32[64,1,1024]{2,1,0:T(1,128)} reshape(f32[64,32,32]{2,1,0:T(8,128)} %copy.98) | data formatting | bytes 524288
  152.6 9.0 %all-to-all-done.5 = f32[64,32,1]{1,2,0:T(1,128)S(1)} async-done(((f32[64,32,1]{1,2,0:T(1,128)}), f32[64,32,1]{1,2,0:T(1,128)S(1)}, u32[]{:S(2)}, u32[]{:S(2)}) %all-to-all-start.5) | async-done | bytes 8224 | tf_op jit(solution)/shard_map/all_to_all | solution.py:46
  161.6 5.7 %all-to-all-start.4 = ((f32[64,1,1024]{2,1,0:T(1,128)}), f32[64,1,1024]{2,1,0:T(1,128)S(1)}, u32[]{:S(2)}, u32[]{:S(2)}) async-start(f32[64,1,1024]{2,1,0:T(1,128)} %reshape.1678), calls=%async_computation.4 | async-start | bytes 524288 | tf_op jit(solution)/shard_map/all_to_all | solution.py:46
  167.4 18.8 %all-to-all-done.4 = f32[64,1,1024]{2,1,0:T(1,128)S(1)} async-done(((f32[64,1,1024]{2,1,0:T(1,128)}), f32[64,1,1024]{2,1,0:T(1,128)S(1)}, u32[]{:S(2)}, u32[]{:S(2)}) %all-to-all-start.4) | async-done | bytes 262176 | tf_op jit(solution)/shard_map/all_to_all | solution.py:46
  186.2 1.3 reduce.42
  188.4 22.5 %all_to_all.47 = bf16[64,2,512]{2,1,0:T(2,128)(2,1)S(1)} all-to-all(bf16[64,2,512]{2,1,0:T(2,128)(2,1)S(1)} %reshape.1680), channel_id=1, replica_groups=mesh['kv_0'=16,'kv_1'=4,'tp'=8] {'kv_0','kv_1'}, dimensions={0} | all-to-all | bytes 262144 | tf_op jit(solution)/shard_map/all_to_all | solution.py:31
  212.4 10.8 %all_to_all.48 = f32[8,1,2048]{2,1,0:T(1,128)S(1)} all-to-all(f32[8,1,2048]{2,1,0:T(1,128)S(1)} %reshape.1682), channel_id=1, replica_groups=mesh['kv_0'=16,'kv_1'=4,'tp'=8] {'tp'}, dimensions={0} | all-to-all | bytes 131072 | tf_op jit(solution)/shard_map/all_to_all | solution.py:31
  223.2 0.8 reduce.43
  (124 shorter events, 14.8 us)
Async XLA Ops:
  0.0 67.4 %copy-start = (bf16[32,2,128,128]{3,2,1,0:T(8,128)(2,1)S(1)}, bf16[32,2,128,128]{3,2,1,0:T(8,128)(2,1)}, u32[]{:S(2)}) copy-start(bf16[32,2,128,128]{3,2,1,0:T(8,128)(2,1)} %param.21) | copy-start | bytes 6291460
  40.7 21.3 %all-to-all-start.1 = ((f32[64,1,386]{2,1,0:T(1,128)}), f32[64,1,386]{2,1,0:T(1,128)S(1)}, u32[]{:S(2)}, u32[]{:S(2)}) async-start(f32[64,1,386]{2,1,0:T(1,128)} %broadcast_in_dim.32), calls=%async_computation.1 | async-start | bytes 262144 | tf_op jit(solution)/shard_map/all_to_all | solution.py:31
  66.2 2.4 %copy-start.5 = (f32[32,2,128]{2,1,0:T(2,128)S(1)}, f32[32,2,128]{2,1,0:T(2,128)}, u32[]{:S(2)}) copy-start(f32[32,2,128]{2,1,0:T(2,128)} %param.23) | copy-start | bytes 98308
  71.5 55.1 %copy-start.4 = (bf16[256,64]{0,1:T(8,128)(2,1)S(1)}, bf16[256,64]{0,1:T(8,128)(2,1)}, u32[]{:S(2)}) copy-start(bf16[256,64]{0,1:T(8,128)(2,1)} %param.26) | copy-start | bytes 98308
  94.4 46.1 %copy-start.1 = (bf16[32,64]{1,0:T(8,128)(2,1)S(1)}, bf16[32,64]{1,0:T(8,128)(2,1)}, u32[]{:S(2)}) copy-start(bf16[32,64]{1,0:T(8,128)(2,1)} %param.15) | copy-start | bytes 12292
  94.5 53.6 %copy-start.2 = (bf16[64,2048]{1,0:T(8,128)(2,1)S(1)}, bf16[64,2048]{1,0:T(8,128)(2,1)}, u32[]{:S(2)}) copy-start(bf16[64,2048]{1,0:T(8,128)(2,1)} %param.28) | copy-start | bytes 786436
  108.3 21.9 %all-to-all-start.2 = ((f32[8,1,32]{2,1,0:T(1,128)}), f32[8,1,32]{2,1,0:T(1,128)S(1)}, u32[]{:S(2)}, u32[]{:S(2)}) async-start(f32[8,1,32]{2,1,0:T(1,128)} %broadcast_in_dim.35), calls=%async_computation.2 | async-start | bytes 8192 | tf_op jit(solution)/shard_map/all_to_all | solution.py:31
  130.2 8.8 %all-to-all-start.3 = ((f32[8,1,2048]{2,1,0:T(1,128)}), f32[8,1,2048]{2,1,0:T(1,128)S(1)}, u32[]{:S(2)}, u32[]{:S(2)}) async-start(f32[8,1,2048]{2,1,0:T(1,128)} %reshape.1676), calls=%async_computation.3 | async-start | bytes 131072 | tf_op jit(solution)/shard_map/all_to_all | solution.py:31
  141.3 20.3 %all-to-all-start.5 = ((f32[64,32,1]{1,2,0:T(1,128)}), f32[64,32,1]{1,2,0:T(1,128)S(1)}, u32[]{:S(2)}, u32[]{:S(2)}) async-start(f32[64,32,1]{1,2,0:T(1,128)} %transpose.61), calls=%async_computation.5 | async-start | bytes 65536 | tf_op jit(solution)/shard_map/all_to_all | solution.py:46
  161.6 24.5 %all-to-all-start.4 = ((f32[64,1,1024]{2,1,0:T(1,128)}), f32[64,1,1024]{2,1,0:T(1,128)S(1)}, u32[]{:S(2)}, u32[]{:S(2)}) async-start(f32[64,1,1024]{2,1,0:T(1,128)} %reshape.1678), calls=%async_computation.4 | async-start | bytes 524288 | tf_op jit(solution)/shard_map/all_to_all | solution.py:46
  187.9 24.1 %copy-start.3 = (bf16[2048,64]{0,1:T(8,128)(2,1)S(1)}, bf16[2048,64]{0,1:T(8,128)(2,1)}, u32[]{:S(2)}) copy-start(bf16[2048,64]{0,1:T(8,128)(2,1)} %param.29) | copy-start | bytes 786436
where the time goes:
time: 226 us; the launch traced here: 225 us
  blocking collectives  99.7 us (44%)
  waiting for transfers between devices  48.3 us (21%)
  starting transfers between devices  40 us (18%)
  local copies, waits for them, and re-layouts  18.2 us (8%)
  other arithmetic  10.4 us (5%)
  matrix products  7.55 us (3%)
    all_to_all x1, blocking collectives, sum_at_owner(): lax.all_to_all(cut_along(value, dim, devices), axis, 0, 0, tiled=True)  34.1 us
    all_to_all x2, blocking collectives, sent_to_all(): return lax.all_to_all(copies, axis, split_axis=0, concat_axis=0, tiled=True)  33.3 us
    all_gather x2, blocking collectives, all_in_one(): both, at, found = (lax.all_gather(jnp.concatenate(lines), axis), 0, {})  32.3 us
    all_to_all x2, waiting for transfers between devices, sum_at_owner(): lax.all_to_all(cut_along(value, dim, devices), axis, 0, 0, tiled=True)  27.8 us
    all_to_all x3, starting transfers between devices, sent_to_all(): return lax.all_to_all(copies, axis, split_axis=0, concat_axis=0, tiled=True)  27.6 us
    all_to_all x3, waiting for transfers between devices, sent_to_all(): return lax.all_to_all(copies, axis, split_axis=0, concat_axis=0, tiled=True)  20.5 us
    all_to_all x2, starting transfers between devices, sum_at_owner(): lax.all_to_all(cut_along(value, dim, devices), axis, 0, 0, tiled=True)  12.4 us
    unnamed x24, local copies, waits for them, and re-layouts  4.64 us
  transfers between devices with their start and end apart: 5, of which 5 were waited for; matrix products, arithmetic and copies ran while one was open for 4% of the time, Pallas kernels for 0%

commit v1 on v0

v1 whole, which is shorter than its diff:
```python
import math

import jax
import jax.numpy as jnp
from jax import lax
from jax.experimental import pallas as pl
from jax.experimental.pallas import tpu as pltpu
from jax.sharding import Mesh
from jax.sharding import PartitionSpec as P

KV = ("z", "y")
norm_eps = 1e-06
masked_score = -1e30
F32 = jnp.float32
BF16 = jnp.bfloat16
WIDTH = 4096
HEADS_WIDTH = 2048


def swap(value, axis):
    return lax.all_to_all(value, axis, split_axis=0, concat_axis=0, tiled=True)


def dot(a, b):
    return jnp.dot(a, b, preferred_element_type=F32)


def dot_nt(a, b):
    return lax.dot_general(a, b, (((1,), (1,)), ((), ())), preferred_element_type=F32)


def lanes(rows):
    return lax.broadcasted_iota(jnp.int32, (rows, 128), 1)


def row_is(count, index):
    return lax.broadcasted_iota(jnp.int32, (count, 1), 0) == index


def high(value):
    return value.astype(BF16).astype(F32)


def columns(values):
    lane = lanes(values[0].shape[0])
    tile = jnp.zeros(lane.shape, F32)
    for k, value in enumerate(values):
        tile = jnp.where(lane == k, value, tile)
    return tile


def project(stream, gain_in, gain_mlp, w_query, w_key, w_value, w_forget, out, gate_rows, sem):
    kv = lax.axis_index("z") * 4 + lax.axis_index("y")
    head = lax.axis_index("tp") * 2
    start = pl.multiple_of((kv // 2) * 128, 128)
    copy = pltpu.make_async_copy(w_forget.at[:, pl.ds(start, 128)], gate_rows, sem)
    copy.start()
    x = stream[...].astype(F32)
    scaled = (x * gain_in[...].astype(F32)).astype(BF16)
    squares = jnp.sum(x * x, axis=1, keepdims=True)
    for k, w in enumerate((w_query, w_key, w_value)):
        part = dot(scaled, w[...])
        for y in range(4):
            for h in range(2):
                out[y, k * 16 + h * 8 : k * 16 + h * 8 + 8, :] = part[y * 8 : y * 8 + 8, h * 128 : h * 128 + 128]
    copy.wait()
    wide = jnp.concatenate([scaled, scaled], axis=1)
    wide = jnp.where(lanes(32) // 64 == kv % 2, wide.astype(F32), 0.0).astype(BF16)
    gates = dot_nt(wide, gate_rows[...])
    column = lax.broadcasted_iota(jnp.int32, gates.shape, 1)
    first = jnp.sum(jnp.where(column == head, gates, 0.0), axis=1, keepdims=True)
    second = jnp.sum(jnp.where(column == head + 1, gates, 0.0), axis=1, keepdims=True)
    gain = gain_mlp[...].astype(F32)
    gain = jnp.broadcast_to(jnp.concatenate([gain, gain], axis=1), (32, 128))
    extra = jnp.where(lanes(32) < 64, columns([squares, first, second]), gain)
    twice = jnp.concatenate([x, x], axis=1)
    for y in range(4):
        out[y, 48:56, :] = extra[y * 8 : y * 8 + 8]
        out[y, 56:64, :] = twice[y * 8 : y * 8 + 8]


def spread_rows(got, out, stream_all, gain_all):
    total = got[0, 0:56] + got[1, 0:56] + got[2, 0:56] + got[3, 0:56]
    q = total[0:16].astype(BF16)
    x = jnp.where(lanes(8) < 3, total[48:56], 0.0)
    one = high(x)
    two = high(x - one)
    three = high(x - one - two)
    extra = one + pltpu.roll(two, 4, 1) + pltpu.roll(three, 8, 1)
    row = lax.broadcasted_iota(jnp.int32, (8, 128), 0)
    for p in range(16):
        k = total[16 + p : 17 + p]
        v = total[32 + p : 33 + p]
        own = jnp.where(row == 0, k, jnp.where(row == 1, v, 0.0))
        out[p, 0:16, :] = q
        out[p, 16:32, :] = jnp.concatenate([extra, own], axis=0).astype(BF16)
    left = lanes(8) < 64
    for k in range(2):
        stream_all[k] = jnp.where(left, got[2 * k, 56:64], got[2 * k + 1, 56:64])
        gain_all[k] = jnp.where(left, pltpu.roll(got[2 * k, 48:56], 64, 1), got[2 * k + 1, 48:56])


def finish_rows(got, w_out, out, own_out):
    z = lax.axis_index("z")
    total = got[0].astype(F32)
    for k in range(1, 16):
        total = total + got[k].astype(F32)
    x = total[16:24]
    x = x + pltpu.roll(x, 124, 1) + pltpu.roll(x, 120, 1)
    scale = lax.rsqrt(x[:, 0:1] / WIDTH + norm_eps)
    scale = jnp.concatenate([scale, scale], axis=0)
    gate = jnp.concatenate([x[:, 1:2], x[:, 2:3]], axis=0) * scale
    q = (total[0:16] * scale).astype(BF16)
    mine = row_is(16, z)
    scale_z = jnp.sum(jnp.where(mine, scale, 0.0), axis=0, keepdims=True)
    gate_z = jnp.sum(jnp.where(mine, gate, 0.0), axis=0, keepdims=True)
    k = high(total[24:25] * scale_z)
    v = high(total[25:26] * scale_z)
    q_z = jnp.sum(jnp.where(mine, q.astype(F32), 0.0), axis=0, keepdims=True)
    own = jnp.sum(q_z * k, axis=1, keepdims=True) * (1.0 / math.sqrt(128))
    own = own + jnp.maximum(-gate_z, 0.0) + jnp.log1p(jnp.exp(-jnp.abs(gate_z)))
    row = lax.broadcasted_iota(jnp.int32, (8, 128), 0)
    own_out[...] = jnp.where(row == 0, own, v)
    w = w_out[...]
    for y in range(4):
        out[y, 0:16, :] = q
        out[y, 16:80, :] = w[:, 0:128]
        out[y, 80:144, :] = w[:, 128:256]


def attend(q, keys, values, decay, lengths, first):
    q = q.reshape(4, 2, 8, 128).swapaxes(1, 2).reshape(32, 2, 128)
    s = jnp.einsum("shd,shpd->shp", q, keys, preferred_element_type=F32)
    s = s * (1.0 / math.sqrt(128)) + decay
    live = (first + lax.iota(jnp.int32, 128)[None, :] < lengths[:, None])[:, None, :]
    s = jnp.where(live, s, masked_score)
    peak = jnp.max(s, axis=2, keepdims=True)
    probs = jnp.where(live, jnp.exp(s - peak), 0.0)
    total = jnp.sum(probs, axis=2, keepdims=True)
    out = jnp.einsum("shp,shpd->shd", probs.astype(BF16), values, preferred_element_type=F32)
    lane = lax.broadcasted_iota(jnp.int32, (32, 2, 128), 2)
    extra = jnp.where(lane == 0, peak, total)
    both = jnp.stack([out, extra]).reshape(2, 4, 8, 2, 128)
    return both.transpose(1, 0, 3, 2, 4).reshape(4, 32, 128)


def merge_blocks(got, own, out):
    z = lax.axis_index("z")
    peaks = [got[k, 16:32, 0:1] for k in range(4)]
    totals = [got[k, 16:32, 1:2] for k in range(4)]
    mine = row_is(16, z)
    own_peak = jnp.where(mine, own[0:1, 0:1], masked_score)
    top = own_peak
    for peak in peaks:
        top = jnp.maximum(top, peak)
    own_weight = jnp.where(mine, jnp.exp(own_peak - top), 0.0)
    total = own_weight
    merged = own_weight * own[1:2, :]
    for k in range(4):
        weight = jnp.exp(peaks[k] - top)
        total = total + weight * totals[k]
        merged = merged + weight * got[k, 0:16]
    one = high(top)
    two = high(top - one)
    three = top - one - two
    four = high(total)
    five = total - four
    parts = []
    for h in range(2):
        for value in (one, two, three, four, five):
            parts.append(value[h * 8 : h * 8 + 8])
    extra = columns(parts).astype(BF16)
    merged = merged.astype(BF16)
    for k in range(16):
        out[k, 0:16, :] = merged
        out[k, 16:24, :] = extra


def project_out(got, w_all, gain_att, out):
    gain = gain_att[...].astype(F32)
    squares = jnp.zeros((8, 1), F32)
    part = jnp.zeros((8, 256), F32)
    extras = [got[k, 16:24, :].astype(F32) for k in range(16)]
    for h in range(2):
        c = h * 5
        peaks = [e[:, c : c + 1] + e[:, c + 1 : c + 2] + e[:, c + 2 : c + 3] for e in extras]
        top = peaks[0]
        for peak in peaks[1:]:
            top = jnp.maximum(top, peak)
        total = jnp.zeros((8, 1), F32)
        merged = jnp.zeros((8, 128), F32)
        for k in range(16):
            weight = jnp.exp(peaks[k] - top)
            total = total + weight * (extras[k][:, c + 3 : c + 4] + extras[k][:, c + 4 : c + 5])
            merged = merged + weight * got[k, 0:16, :].astype(F32)[h * 8 : h * 8 + 8]
        attended = merged / total
        squares = squares + jnp.sum(attended * attended, axis=1, keepdims=True)
        attended_in = (attended * gain[:, h * 128 : h * 128 + 128]).astype(BF16)
        w = jnp.concatenate([w_all[y, 16 + h * 64 : 80 + h * 64, :] for y in range(4)], axis=0)
        part = part + dot_nt(attended_in, w)
    extra = columns([squares])
    for k in range(8):
        out[k, 0:8, :] = part[:, 0:128]
        out[k, 8:16, :] = part[:, 128:256]
        out[k, 16:24, :] = extra


def mix_up(got, stream_all, gain_all, w0, w1, w2, w3, out, residual_out, halves):
    y = lax.axis_index("y")
    total = got[0]
    for k in range(1, 8):
        total = total + got[k]
    scale = lax.rsqrt(total[16:24, 0:1] / HEADS_WIDTH + norm_eps)
    squares = jnp.zeros((8, 1), F32)
    for k in range(2):
        residual = high(stream_all[k] + scale * total[k * 8 : k * 8 + 8])
        squares = squares + jnp.sum(residual * residual, axis=1, keepdims=True)
        mixer_in = high(residual * gain_all[k])
        halves[2 * k] = mixer_in
        halves[2 * k + 1] = pltpu.roll(mixer_in, 64, 1)
        residual_out[2 * k] = residual
        residual_out[2 * k + 1] = pltpu.roll(residual, 64, 1)
    up = jnp.zeros((8, 2048), F32)
    for d, w in enumerate((w0, w1, w2, w3)):
        lhs = halves[(y + 4 - d) % 4][:, 0:64].astype(BF16)
        up = up + dot(lhs, w[...])
    one = high(squares)
    two = high(squares - one)
    extra = columns([one, two, squares - one - two])
    for k in range(16):
        both = jnp.concatenate([up[:, k * 128 : k * 128 + 128], extra], axis=0)
        out[k] = both.astype(BF16)


def activate(got, out):
    total = got[0].astype(F32)
    for k in range(1, 16):
        total = total + got[k].astype(F32)
    squares = total[8:16, 0:1] + total[8:16, 1:2] + total[8:16, 2:3]
    scale = lax.rsqrt(squares / WIDTH + norm_eps)
    hidden = jnp.square(jnp.maximum(total[0:8] * scale, 0.0)).astype(BF16)
    for k in range(16):
        out[k] = hidden


def mix_down(got, residual, w0, w1, w2, w3, out):
    y = lax.axis_index("y")
    t = lax.axis_index("tp")
    hidden = jnp.concatenate([got[k] for k in range(16)], axis=1)
    for d, w in enumerate((w0, w1, w2, w3)):
        source = (y + 4 - d) % 4
        part = dot_nt(hidden, w[...])
        part = jnp.concatenate([part, part], axis=1)
        part = part + jnp.where(t == 0, residual[source], 0.0)
        for k in range(8):
            out[source * 8 + k] = part


def finish(got, out):
    for y in range(4):
        total = got[y * 8]
        for k in range(1, 8):
            total = total + got[y * 8 + k]
        out[y * 8 : y * 8 + 8, :] = total[:, 0:64].astype(BF16)


def call(kernel, outs, *args, anywhere=(), scratch=()):
    specs = [
        pl.BlockSpec(memory_space=pl.ANY) if k in anywhere else pl.BlockSpec(memory_space=pltpu.VMEM)
        for k in range(len(args))
    ]
    shapes = [jax.ShapeDtypeStruct(s, d) for s, d in outs]
    found = pl.pallas_call(
        kernel,
        out_shape=shapes,
        in_specs=specs,
        out_specs=[pl.BlockSpec(memory_space=pltpu.VMEM) for _ in shapes],
        scratch_shapes=list(scratch),
        name=kernel.__name__,
    )(*args)
    return found if len(shapes) > 1 else found[0]


def around(value):
    n = lax.axis_size("y")
    moved = [lax.ppermute(value, "y", [(k, (k + d) % n) for k in range(n)]) for d in range(1, n)]
    return [value, *moved]


def per_device(
    stream,
    gain_in,
    w_query,
    w_key,
    w_value,
    w_forget,
    keys_cache,
    values_cache,
    decay_cache,
    lengths,
    gain_att,
    w_out,
    gain_mlp,
    w_up,
    w_down,
):
    kv = lax.axis_index(KV)
    lines = call(
        project,
        [((4, 64, 128), F32)],
        stream,
        gain_in.reshape(1, 64),
        gain_mlp.reshape(1, 64),
        w_query,
        w_key,
        w_value,
        w_forget.T,
        anywhere=(6,),
        scratch=(pltpu.VMEM((16, 128), BF16), pltpu.SemaphoreType.DMA),
    )
    got = swap(lines, "y")
    lines, stream_all, gain_all = call(
        spread_rows, [((16, 32, 128), BF16), ((2, 8, 128), F32), ((2, 8, 128), F32)], got
    )
    lines, w_up, w_down = lax.optimization_barrier((lines, w_up, w_down))
    got = swap(lines, "z")
    ups = around(w_up)
    downs = around(w_down.T)
    lines, own = call(finish_rows, [((4, 144, 128), BF16), ((8, 128), F32)], got, w_out.T)
    w_all = swap(lines, "y")
    got = swap(attend(w_all[:, 0:16], keys_cache, values_cache, decay_cache, lengths, kv * 128), "y")
    lines = call(merge_blocks, [((16, 24, 128), BF16)], got, own)
    got = swap(lines, "z")
    lines = call(project_out, [((8, 24, 128), F32)], got, w_all, gain_att.reshape(1, 256))
    got = swap(lines, "tp")
    lines, residual = call(
        mix_up,
        [((16, 16, 128), BF16), ((4, 8, 128), F32)],
        got,
        stream_all,
        gain_all,
        *ups,
        scratch=(pltpu.VMEM((4, 8, 128), F32),),
    )
    got = swap(lines, "z")
    got = swap(call(activate, [((16, 8, 128), BF16)], got), "z")
    lines = call(mix_down, [((32, 8, 128), F32)], got, residual, *downs)
    got = swap(lines, ("y", "tp"))
    return call(finish, [((32, 64), BF16)], got)


def solution(mesh):
    split = Mesh(mesh.devices.reshape(16, 4, mesh.shape["tp"]), ("z", "y", "tp"))
    return jax.shard_map(
        per_device,
        mesh=split,
        in_specs=(
            P(None, KV),
            P(KV),
            P(KV, "tp"),
            P(KV, "tp"),
            P(KV, "tp"),
            P(),
            P(None, "tp", KV, None),
            P(None, "tp", KV, None),
            P(None, "tp", KV),
            P(),
            P("tp"),
            P("tp", KV),
            P(KV),
            P(KV, "tp"),
            P("tp", KV),
        ),
        out_specs=P(None, KV),
        check_vma=False,
    )
```

time: 226 us -> 169 us (0.75)
  blocking collectives: 99.7 us -> 33 us
  starting transfers between devices: 40 us -> 71.4 us
  Pallas kernels: 0 us -> 17.5 us
  local copies, waits for them, and re-layouts: 18.2 us -> 4.62 us
  waiting for transfers between devices: 48.3 us -> 36 us
  other arithmetic: 10.4 us -> 1.16 us
  matrix products: 7.55 us -> 3.45 us
    all_to_all x3, blocking collectives: 67.5 us -> 33 us  [swap(): return lax.all_to_all(value, axis, split_axis=0, concat_axis=0, tiled=True)]
    all_gather x2 -> x0, blocking collectives: 32.3 us -> none  [all_in_one(): both, at, found = (lax.all_gather(jnp.concatenate(lines), axis), 0, {})]
    ppermute x0 -> x6, starting transfers between devices: none -> 18.6 us  [around(): lax.ppermute(value, 'y', [(k, (k + d) % n) for k in range(n)])]
    pallas_call x0 -> x9, Pallas kernels: none -> 17.5 us  [call(): pl.pallas_call(kernel, out_shape=shapes, in_specs=specs, out_specs=[pl.Bl...]
    all_to_all x5 -> x6, starting transfers between devices: 40 us -> 52.9 us  [swap(): return lax.all_to_all(value, axis, split_axis=0, concat_axis=0, tiled=True)]
    all_to_all x5 -> x6, waiting for transfers between devices: 48.3 us -> 36 us  [swap(): return lax.all_to_all(value, axis, split_axis=0, concat_axis=0, tiled=True)]
    dot_general x9 -> x2, matrix products: 7.55 us -> 3.45 us  [the longest x1 2.28 us: attend(): jnp.einsum('shp,shpd->shd', probs.astype(BF16), values, preferred_element...]
    slice x6 -> x0, local copies, waits for them, and re-layouts: 3.79 us -> none  [the longest x3 3.75 us: together(): finished.append(so_far[at:at + a.size].reshape(a.shape))]
  transfers between devices with their start and end apart: 5 -> 12, of which waited for: 5 -> 6; matrix products, arithmetic and copies ran while one was open for 4% -> 1% of each run, Pallas kernels for 0% -> 2%
where the time goes in v1:
time: 169 us; the launch traced here: 167 us
  starting transfers between devices  71.4 us (42%)
  waiting for transfers between devices  36 us (21%)
  blocking collectives  33 us (20%)
  Pallas kernels  17.5 us (10%)
  local copies, waits for them, and re-layouts  4.62 us (3%)
  matrix products  3.45 us (2%)
    all_to_all x6, starting transfers between devices, swap(): return lax.all_to_all(value, axis, split_axis=0, concat_axis=0, tiled=True)  52.9 us
    all_to_all x6, waiting for transfers between devices, swap(): return lax.all_to_all(value, axis, split_axis=0, concat_axis=0, tiled=True)  36 us
    all_to_all x3, blocking collectives, swap(): return lax.all_to_all(value, axis, split_axis=0, concat_axis=0, tiled=True)  33 us
    ppermute x6, starting transfers between devices, around(): lax.ppermute(value, 'y', [(k, (k + d) % n) for k in range(n)])  18.6 us
    pallas_call x9, Pallas kernels, call(): pl.pallas_call(kernel, out_shape=shapes, in_specs=specs, out_specs=[pl.Bl...  17.5 us
  transfers between devices with their start and end apart: 12, of which 6 were waited for; matrix products, arithmetic and copies ran while one was open for 1% of the time, Pallas kernels for 2%

profile of v1, /device:TPU:1, one launch (start us, length us, event | category | flops | bytes accessed | tf_op | source)
XLA Modules:
  0.0 167.4 jit_solution(4373454670068128633)
XLA Ops:
  0.0 2.6 %project.1 = f32[4,64,128]{2,1,0:T(8,128)} custom-call(bf16[32,64]{1,0:T(8,128)(2,1)} %stream.1, bf16[1,64]{1,0:T(2,128)(2,1)} %bitcast.42, bf16[1,64]{1,0:T(2,128)(2,1)} %bitcast.43, bf16[64,256]{1,0:T(8,128)(2,1)} %w_query.1, bf16[64,256]{1,0:T(8,128)(2,1)} %w_key.1, bf16[64,256]{1,0:T(8,128)(2,1)} %w_value.1, bf16[16,4096]{1,0:T(8,128)(2,1)} %bitcast.38), custom_call_target="tpu_custom_call" | custom-call | tf_op jit(solution)/shard_map/project/pallas_call | solution.py:273
  2.7 9.9 %all_to_all.45.got = f32[4,64,128]{2,1,0:T(8,128)} all-to-all(f32[4,64,128]{2,1,0:T(8,128)} %project.1), channel_id=1, replica_groups=mesh['z'=16,'y'=4,'tp'=8] {'y'}, dimensions={0} | all-to-all | bytes 262144 | tf_op jit(solution)/shard_map/all_to_all | solution.py:21
  12.6 1.6 spread_rows.1
  14.2 14.9 %all-to-all-start.1 = ((bf16[16,32,128]{2,1,0:T(8,128)(2,1)}), bf16[16,32,128]{2,1,0:T(8,128)(2,1)S(1)}, u32[]{:S(2)}, u32[]{:S(2)}) async-start(bf16[16,32,128]{2,1,0:T(8,128)(2,1)} %get-tuple-element.16), calls=%async_computation.1 | async-start | bytes 262144 | tf_op jit(solution)/shard_map/all_to_all | solution.py:21
  29.9 11.2 %all-to-all-done.1.got = bf16[16,32,128]{2,1,0:T(8,128)(2,1)S(1)} async-done(((bf16[16,32,128]{2,1,0:T(8,128)(2,1)}), bf16[16,32,128]{2,1,0:T(8,128)(2,1)S(1)}, u32[]{:S(2)}, u32[]{:S(2)}) %all-to-all-start.1) | async-done | bytes 131104 | tf_op jit(solution)/shard_map/all_to_all | solution.py:21
  41.8 1.8 %finish_rows.1 = (bf16[4,144,128]{2,1,0:T(8,128)(2,1)}, f32[8,128]{1,0:T(8,128)}) custom-call(bf16[16,32,128]{2,1,0:T(8,128)(2,1)} %copy-done.2, bf16[64,256]{1,0:T(8,128)(2,1)} %bitcast.41), custom_call_target="tpu_custom_call" | custom-call | tf_op jit(solution)/shard_map/finish_rows/pallas_call | solution.py:273
  43.6 3.3 %all-to-all-start.2 = ((bf16[4,144,128]{2,1,0:T(8,128)(2,1)}), bf16[4,144,128]{2,1,0:T(8,128)(2,1)S(1)}, u32[]{:S(2)}, u32[]{:S(2)}) async-start(bf16[4,144,128]{2,1,0:T(8,128)(2,1)} %get-tuple-element.17), calls=%async_computation.2 | async-start | bytes 294912 | tf_op jit(solution)/shard_map/all_to_all | solution.py:21
  47.0 4.9 %all-to-all-done.2.w_all = bf16[4,144,128]{2,1,0:T(8,128)(2,1)S(1)} async-done(((bf16[4,144,128]{2,1,0:T(8,128)(2,1)}), bf16[4,144,128]{2,1,0:T(8,128)(2,1)S(1)}, u32[]{:S(2)}, u32[]{:S(2)}) %all-to-all-start.2) | async-done | bytes 147488 | tf_op jit(solution)/shard_map/all_to_all | solution.py:21
  53.6 2.3 %fusion = f32[32,2,1,128]{3,2,1,0:T(1,128)S(1)} fusion(bf16[32,2,128,128]{3,2,1,0:T(8,128)(2,1)} %param.22, bf16[32,2,128,1]{2,1,0,3:T(2,128)(2,1)S(1)} %get-tuple-element.25), kind=kOutput, calls=%fused_computation.2 | convolution fusion | flops 2097152 | bytes 2146304 | tf_op jit(solution)/shard_map/shp,shpd->shd/dot_general | solution.py:140
  56.0 7.5 %all_to_all.46.got = f32[4,32,128]{2,1,0:T(8,128)} all-to-all(f32[4,32,128]{2,1,0:T(8,128)S(1)} %bitcast.36), channel_id=1, replica_groups=mesh['z'=16,'y'=4,'tp'=8] {'y'}, dimensions={0} | all-to-all | bytes 131072 | tf_op jit(solution)/shard_map/all_to_all | solution.py:21
  63.5 1.6 merge_blocks.1
  65.1 4.0 %all-to-all-start.4 = ((bf16[16,24,128]{2,1,0:T(8,128)(2,1)}), bf16[16,24,128]{2,1,0:T(8,128)(2,1)S(1)}, u32[]{:S(2)}, u32[]{:S(2)}) async-start(bf16[16,24,128]{2,1,0:T(8,128)(2,1)} %merge_blocks.1), calls=%async_computation.4 | async-start | bytes 196608 | tf_op jit(solution)/shard_map/all_to_all | solution.py:21
  69.2 2.2 %collective-permute-start = (bf16[64,2048]{1,0:T(8,128)(2,1)S(1)}, bf16[64,2048]{1,0:T(8,128)(2,1)S(1)}, u32[]{:S(2)}, u32[]{:S(2)}) collective-permute-start(bf16[64,2048]{1,0:T(8,128)(2,1)S(1)} %copy-done.10), channel_id=1, source_target_pairs={{0,8},{8,16},{16,24},{24,0},{1,9},{9,17},{17,25},{25,1},{2,10},{10... | collective-permute-start | bytes 786440 | tf_op jit(solution)/shard_map/ppermute | solution.py:286
  71.4 3.7 %collective-permute-start.1 = (bf16[64,2048]{1,0:T(8,128)(2,1)S(1)}, bf16[64,2048]{1,0:T(8,128)(2,1)S(1)}, u32[]{:S(2)}, u32[]{:S(2)}) collective-permute-start(bf16[64,2048]{1,0:T(8,128)(2,1)S(1)} %copy-done.10), channel_id=1, source_target_pairs={{0,16},{8,24},{16,0},{24,8},{1,17},{9,25},{17,1},{25,9},{2,18},{10... | collective-permute-start | bytes 786440 | tf_op jit(solution)/shard_map/ppermute | solution.py:286
  75.1 2.6 %collective-permute-start.2 = (bf16[64,2048]{1,0:T(8,128)(2,1)S(1)}, bf16[64,2048]{1,0:T(8,128)(2,1)S(1)}, u32[]{:S(2)}, u32[]{:S(2)}) collective-permute-start(bf16[64,2048]{1,0:T(8,128)(2,1)S(1)} %copy-done.10), channel_id=1, source_target_pairs={{0,24},{8,0},{16,8},{24,16},{1,25},{9,1},{17,9},{25,17},{2,26},{10... | collective-permute-start | bytes 786440 | tf_op jit(solution)/shard_map/ppermute | solution.py:286
  77.7 1.2 reshape.63.gain_att
  78.9 2.1 %all-to-all-done.4.got = bf16[16,24,128]{2,1,0:T(8,128)(2,1)S(1)} async-done(((bf16[16,24,128]{2,1,0:T(8,128)(2,1)}), bf16[16,24,128]{2,1,0:T(8,128)(2,1)S(1)}, u32[]{:S(2)}, u32[]{:S(2)}) %all-to-all-start.4) | async-done | bytes 98336 | tf_op jit(solution)/shard_map/all_to_all | solution.py:21
  81.6 2.0 %project_out.1 = f32[8,24,128]{2,1,0:T(8,128)} custom-call(bf16[16,24,128]{2,1,0:T(8,128)(2,1)} %copy-done.4, bf16[4,144,128]{2,1,0:T(8,128)(2,1)} %copy-done.1, bf16[1,256]{1,0:T(2,128)(2,1)} %reshape.63.gain_att), custom_call_target="tpu_custom_call" | custom-call | tf_op jit(solution)/shard_map/project_out/pallas_call | solution.py:273
  83.6 11.3 %all-to-all-start.5 = ((f32[8,24,128]{2,1,0:T(8,128)}), f32[8,24,128]{2,1,0:T(8,128)S(1)}, u32[]{:S(2)}, u32[]{:S(2)}) async-start(f32[8,24,128]{2,1,0:T(8,128)} %project_out.1), calls=%async_computation.5 | async-start | bytes 196608 | tf_op jit(solution)/shard_map/all_to_all | solution.py:21
  94.9 4.9 %all-to-all-done.5.got = f32[8,24,128]{2,1,0:T(8,128)S(1)} async-done(((f32[8,24,128]{2,1,0:T(8,128)}), f32[8,24,128]{2,1,0:T(8,128)S(1)}, u32[]{:S(2)}, u32[]{:S(2)}) %all-to-all-start.5) | async-done | bytes 98336 | tf_op jit(solution)/shard_map/all_to_all | solution.py:21
  100.5 2.3 %mix_up.1 = (bf16[16,16,128]{2,1,0:T(8,128)(2,1)}, f32[4,8,128]{2,1,0:T(8,128)}) custom-call(f32[8,24,128]{2,1,0:T(8,128)} %copy-done.3, f32[2,8,128]{2,1,0:T(8,128)} %get-tuple-element.19.stream_all, f32[2,8,128]{2,1,0:T(8,128)} %get-tuple-element.20.gain_all, bf16[64,2048]{1,0:T(8,128)(2,1)} %w0, bf16[64,2048]{1,0:T(8,128)(2,1)} %copy-done.11, ...), custom_call_target="tpu_custom_call" | custom-call | tf_op jit(solution)/shard_map/mix_up/pallas_call | solution.py:273
  102.8 9.3 %all-to-all-start.6 = ((bf16[16,16,128]{2,1,0:T(8,128)(2,1)}), bf16[16,16,128]{2,1,0:T(8,128)(2,1)S(1)}, u32[]{:S(2)}, u32[]{:S(2)}) async-start(bf16[16,16,128]{2,1,0:T(8,128)(2,1)} %get-tuple-element.22), calls=%async_computation.6 | async-start | bytes 131072 | tf_op jit(solution)/shard_map/all_to_all | solution.py:21
  112.2 2.7 %collective-permute-start.3 = (bf16[64,2048]{1,0:T(8,128)(2,1)S(1)}, bf16[64,2048]{1,0:T(8,128)(2,1)S(1)}, u32[]{:S(2)}, u32[]{:S(2)}) collective-permute-start(bf16[64,2048]{1,0:T(8,128)(2,1)S(1)} %bitcast.33), channel_id=1, source_target_pairs={{0,8},{8,16},{16,24},{24,0},{1,9},{9,17},{17,25},{25,1},{2,10},{10... | collective-permute-start | bytes 786440 | tf_op jit(solution)/shard_map/ppermute | solution.py:286
  114.8 3.4 %collective-permute-start.4 = (bf16[64,2048]{1,0:T(8,128)(2,1)S(1)}, bf16[64,2048]{1,0:T(8,128)(2,1)S(1)}, u32[]{:S(2)}, u32[]{:S(2)}) collective-permute-start(bf16[64,2048]{1,0:T(8,128)(2,1)S(1)} %bitcast.34), channel_id=1, source_target_pairs={{0,16},{8,24},{16,0},{24,8},{1,17},{9,25},{17,1},{25,9},{2,18},{10... | collective-permute-start | bytes 786440 | tf_op jit(solution)/shard_map/ppermute | solution.py:286
  118.3 4.0 %collective-permute-start.5 = (bf16[64,2048]{1,0:T(8,128)(2,1)S(1)}, bf16[64,2048]{1,0:T(8,128)(2,1)S(1)}, u32[]{:S(2)}, u32[]{:S(2)}) collective-permute-start(bf16[64,2048]{1,0:T(8,128)(2,1)S(1)} %bitcast.35), channel_id=1, source_target_pairs={{0,24},{8,0},{16,8},{24,16},{1,25},{9,1},{17,9},{25,17},{2,26},{10... | collective-permute-start | bytes 786440 | tf_op jit(solution)/shard_map/ppermute | solution.py:286
  122.2 1.5 all-to-all-done.6.got
  124.4 1.6 activate.1
  126.0 10.0 %all-to-all-start.7 = ((bf16[16,8,128]{2,1,0:T(8,128)(2,1)}), bf16[16,8,128]{2,1,0:T(8,128)(2,1)S(1)}, u32[]{:S(2)}, u32[]{:S(2)}) async-start(bf16[16,8,128]{2,1,0:T(8,128)(2,1)} %activate.1), calls=%async_computation.7 | async-start | bytes 65536 | tf_op jit(solution)/shard_map/all_to_all | solution.py:21
  136.0 11.4 %all-to-all-done.7.got = bf16[16,8,128]{2,1,0:T(8,128)(2,1)S(1)} async-done(((bf16[16,8,128]{2,1,0:T(8,128)(2,1)}), bf16[16,8,128]{2,1,0:T(8,128)(2,1)S(1)}, u32[]{:S(2)}, u32[]{:S(2)}) %all-to-all-start.7) | async-done | bytes 32800 | tf_op jit(solution)/shard_map/all_to_all | solution.py:21
  148.1 2.3 %mix_down.1 = f32[32,8,128]{2,1,0:T(8,128)} custom-call(bf16[16,8,128]{2,1,0:T(8,128)(2,1)} %copy-done.14, f32[4,8,128]{2,1,0:T(8,128)} %get-tuple-element.23.residual, bf16[64,2048]{1,0:T(8,128)(2,1)} %bitcast.32, bf16[64,2048]{1,0:T(8,128)(2,1)} %copy-done.6, bf16[64,2048]{1,0:T(8,128)(2,1)} %copy-done.7, bf16[64,2048]{1,0:T(8,128)(2,1)} %copy-done.8), custom_call_target="tpu_custom_call" | custom-call | tf_op jit(solution)/shard_map/mix_down/pallas_call | solution.py:273
  150.4 15.5 %all_to_all.47.got = f32[32,8,128]{2,1,0:T(8,128)} all-to-all(f32[32,8,128]{2,1,0:T(8,128)} %mix_down.1), channel_id=1, replica_groups=mesh['z'=16,'y'=4,'tp'=8] {'y','tp'}, dimensions={0} | all-to-all | bytes 262144 | tf_op jit(solution)/shard_map/all_to_all | solution.py:21
  165.9 1.5 finish.1
  (51 shorter events, 5.7 us)
Async XLA Ops:
  0.0 51.9 %copy-start = (bf16[32,2,128,128]{3,2,1,0:T(8,128)(2,1)S(1)}, bf16[32,2,128,128]{3,2,1,0:T(8,128)(2,1)}, u32[]{:S(2)}) copy-start(bf16[32,2,128,128]{3,2,1,0:T(8,128)(2,1)} %param.21) | copy-start | bytes 6291460
  0.0 53.0 %copy-start.15 = (f32[32,2,128]{2,1,0:T(2,128)S(1)}, f32[32,2,128]{2,1,0:T(2,128)}, u32[]{:S(2)}) copy-start(f32[32,2,128]{2,1,0:T(2,128)} %param.23) | copy-start | bytes 98308
  14.2 26.9 %all-to-all-start.1 = ((bf16[16,32,128]{2,1,0:T(8,128)(2,1)}), bf16[16,32,128]{2,1,0:T(8,128)(2,1)S(1)}, u32[]{:S(2)}, u32[]{:S(2)}) async-start(bf16[16,32,128]{2,1,0:T(8,128)(2,1)} %get-tuple-element.16), calls=%async_computation.1 | async-start | bytes 262144 | tf_op jit(solution)/shard_map/all_to_all | solution.py:21
  41.1 0.6 copy-start.2
  43.6 8.2 %all-to-all-start.2 = ((bf16[4,144,128]{2,1,0:T(8,128)(2,1)}), bf16[4,144,128]{2,1,0:T(8,128)(2,1)S(1)}, u32[]{:S(2)}, u32[]{:S(2)}) async-start(bf16[4,144,128]{2,1,0:T(8,128)(2,1)} %get-tuple-element.17), calls=%async_computation.2 | async-start | bytes 294912 | tf_op jit(solution)/shard_map/all_to_all | solution.py:21
  51.9 4.0 %copy-start.1 = (bf16[4,144,128]{2,1,0:T(8,128)(2,1)}, bf16[4,144,128]{2,1,0:T(8,128)(2,1)S(1)}, u32[]{:S(2)}) copy-start(bf16[4,144,128]{2,1,0:T(8,128)(2,1)S(1)} %all-to-all-done.2.w_all) | copy-start | bytes 442372
  53.0 16.1 %copy-start.10 = (bf16[64,2048]{1,0:T(8,128)(2,1)S(1)}, bf16[64,2048]{1,0:T(8,128)(2,1)}, u32[]{:S(2)}) copy-start(bf16[64,2048]{1,0:T(8,128)(2,1)} %w0) | copy-start | bytes 786436
  53.6 58.6 %copy-start.5 = (bf16[2048,64]{0,1:T(8,128)(2,1)S(1)}, bf16[2048,64]{0,1:T(8,128)(2,1)}, u32[]{:S(2)}) copy-start(bf16[2048,64]{0,1:T(8,128)(2,1)} %param.29) | copy-start | bytes 786436
  65.1 15.9 %all-to-all-start.4 = ((bf16[16,24,128]{2,1,0:T(8,128)(2,1)}), bf16[16,24,128]{2,1,0:T(8,128)(2,1)S(1)}, u32[]{:S(2)}, u32[]{:S(2)}) async-start(bf16[16,24,128]{2,1,0:T(8,128)(2,1)} %merge_blocks.1), calls=%async_computation.4 | async-start | bytes 196608 | tf_op jit(solution)/shard_map/all_to_all | solution.py:21
  69.2 25.7 %collective-permute-start = (bf16[64,2048]{1,0:T(8,128)(2,1)S(1)}, bf16[64,2048]{1,0:T(8,128)(2,1)S(1)}, u32[]{:S(2)}, u32[]{:S(2)}) collective-permute-start(bf16[64,2048]{1,0:T(8,128)(2,1)S(1)} %copy-done.10), channel_id=1, source_target_pairs={{0,8},{8,16},{16,24},{24,0},{1,9},{9,17},{17,25},{25,1},{2,10},{10... | collective-permute-start | bytes 786440 | tf_op jit(solution)/shard_map/ppermute | solution.py:286
  71.4 23.5 %collective-permute-start.1 = (bf16[64,2048]{1,0:T(8,128)(2,1)S(1)}, bf16[64,2048]{1,0:T(8,128)(2,1)S(1)}, u32[]{:S(2)}, u32[]{:S(2)}) collective-permute-start(bf16[64,2048]{1,0:T(8,128)(2,1)S(1)} %copy-done.10), channel_id=1, source_target_pairs={{0,16},{8,24},{16,0},{24,8},{1,17},{9,25},{17,1},{25,9},{2,18},{10... | collective-permute-start | bytes 786440 | tf_op jit(solution)/shard_map/ppermute | solution.py:286
  75.1 19.8 %collective-permute-start.2 = (bf16[64,2048]{1,0:T(8,128)(2,1)S(1)}, bf16[64,2048]{1,0:T(8,128)(2,1)S(1)}, u32[]{:S(2)}, u32[]{:S(2)}) collective-permute-start(bf16[64,2048]{1,0:T(8,128)(2,1)S(1)} %copy-done.10), channel_id=1, source_target_pairs={{0,24},{8,0},{16,8},{24,16},{1,25},{9,1},{17,9},{25,17},{2,26},{10... | collective-permute-start | bytes 786440 | tf_op jit(solution)/shard_map/ppermute | solution.py:286
  81.0 0.6 copy-start.4
  83.6 16.3 %all-to-all-start.5 = ((f32[8,24,128]{2,1,0:T(8,128)}), f32[8,24,128]{2,1,0:T(8,128)S(1)}, u32[]{:S(2)}, u32[]{:S(2)}) async-start(f32[8,24,128]{2,1,0:T(8,128)} %project_out.1), calls=%async_computation.5 | async-start | bytes 196608 | tf_op jit(solution)/shard_map/all_to_all | solution.py:21
  94.9 5.0 %copy-start.11 = (bf16[64,2048]{1,0:T(8,128)(2,1)}, bf16[64,2048]{1,0:T(8,128)(2,1)S(1)}, u32[]{:S(2)}) copy-start(bf16[64,2048]{1,0:T(8,128)(2,1)S(1)} %collective-permute-done.w1) | copy-start | bytes 786436
  94.9 5.0 %copy-start.12 = (bf16[64,2048]{1,0:T(8,128)(2,1)}, bf16[64,2048]{1,0:T(8,128)(2,1)S(1)}, u32[]{:S(2)}) copy-start(bf16[64,2048]{1,0:T(8,128)(2,1)S(1)} %collective-permute-done.1.w2) | copy-start | bytes 786436
  94.9 5.0 %copy-start.13 = (bf16[64,2048]{1,0:T(8,128)(2,1)}, bf16[64,2048]{1,0:T(8,128)(2,1)S(1)}, u32[]{:S(2)}) copy-start(bf16[64,2048]{1,0:T(8,128)(2,1)S(1)} %collective-permute-done.2.w3) | copy-start | bytes 786436
  99.9 0.6 copy-start.3
  102.8 20.9 %all-to-all-start.6 = ((bf16[16,16,128]{2,1,0:T(8,128)(2,1)}), bf16[16,16,128]{2,1,0:T(8,128)(2,1)S(1)}, u32[]{:S(2)}, u32[]{:S(2)}) async-start(bf16[16,16,128]{2,1,0:T(8,128)(2,1)} %get-tuple-element.22), calls=%async_computation.6 | async-start | bytes 131072 | tf_op jit(solution)/shard_map/all_to_all | solution.py:21
  112.2 23.8 %collective-permute-start.3 = (bf16[64,2048]{1,0:T(8,128)(2,1)S(1)}, bf16[64,2048]{1,0:T(8,128)(2,1)S(1)}, u32[]{:S(2)}, u32[]{:S(2)}) collective-permute-start(bf16[64,2048]{1,0:T(8,128)(2,1)S(1)} %bitcast.33), channel_id=1, source_target_pairs={{0,8},{8,16},{16,24},{24,0},{1,9},{9,17},{17,25},{25,1},{2,10},{10... | collective-permute-start | bytes 786440 | tf_op jit(solution)/shard_map/ppermute | solution.py:286
  114.8 21.2 %collective-permute-start.4 = (bf16[64,2048]{1,0:T(8,128)(2,1)S(1)}, bf16[64,2048]{1,0:T(8,128)(2,1)S(1)}, u32[]{:S(2)}, u32[]{:S(2)}) collective-permute-start(bf16[64,2048]{1,0:T(8,128)(2,1)S(1)} %bitcast.34), channel_id=1, source_target_pairs={{0,16},{8,24},{16,0},{24,8},{1,17},{9,25},{17,1},{25,9},{2,18},{10... | collective-permute-start | bytes 786440 | tf_op jit(solution)/shard_map/ppermute | solution.py:286
  118.3 17.7 %collective-permute-start.5 = (bf16[64,2048]{1,0:T(8,128)(2,1)S(1)}, bf16[64,2048]{1,0:T(8,128)(2,1)S(1)}, u32[]{:S(2)}, u32[]{:S(2)}) collective-permute-start(bf16[64,2048]{1,0:T(8,128)(2,1)S(1)} %bitcast.35), channel_id=1, source_target_pairs={{0,24},{8,0},{16,8},{24,16},{1,25},{9,1},{17,9},{25,17},{2,26},{10... | collective-permute-start | bytes 786440 | tf_op jit(solution)/shard_map/ppermute | solution.py:286
  123.7 0.6 copy-start.9
  126.0 21.4 %all-to-all-start.7 = ((bf16[16,8,128]{2,1,0:T(8,128)(2,1)}), bf16[16,8,128]{2,1,0:T(8,128)(2,1)S(1)}, u32[]{:S(2)}, u32[]{:S(2)}) async-start(bf16[16,8,128]{2,1,0:T(8,128)(2,1)} %activate.1), calls=%async_computation.7 | async-start | bytes 65536 | tf_op jit(solution)/shard_map/all_to_all | solution.py:21
  136.0 11.5 %copy-start.6 = (bf16[64,2048]{1,0:T(8,128)(2,1)}, bf16[64,2048]{1,0:T(8,128)(2,1)S(1)}, u32[]{:S(2)}) copy-start(bf16[64,2048]{1,0:T(8,128)(2,1)S(1)} %collective-permute-done.3.w1) | copy-start | bytes 786436
  136.0 11.4 %copy-start.7 = (bf16[64,2048]{1,0:T(8,128)(2,1)}, bf16[64,2048]{1,0:T(8,128)(2,1)S(1)}, u32[]{:S(2)}) copy-start(bf16[64,2048]{1,0:T(8,128)(2,1)S(1)} %collective-permute-done.4.w2) | copy-start | bytes 786436
  136.0 11.4 %copy-start.8 = (bf16[64,2048]{1,0:T(8,128)(2,1)}, bf16[64,2048]{1,0:T(8,128)(2,1)S(1)}, u32[]{:S(2)}) copy-start(bf16[64,2048]{1,0:T(8,128)(2,1)S(1)} %collective-permute-done.5.w3) | copy-start | bytes 786436
  147.4 0.6 copy-start.14

commit v2 on v1

--- a/solution.py
+++ b/solution.py
@@ -223,7 +223,7 @@
     up = jnp.zeros((8, 2048), F32)
     for d, w in enumerate((w0, w1, w2, w3)):
         lhs = halves[(y + 4 - d) % 4][:, 0:64].astype(BF16)
-        up = up + dot(lhs, w[...])
+        up = up + dot(lhs, w[0:64, :])
     one = high(squares)
     two = high(squares - one)
     extra = columns([one, two, squares - one - two])
@@ -249,7 +249,7 @@
     hidden = jnp.concatenate([got[k] for k in range(16)], axis=1)
     for d, w in enumerate((w0, w1, w2, w3)):
         source = (y + 4 - d) % 4
-        part = dot_nt(hidden, w[...])
+        part = dot_nt(hidden, w[64:128, :])
         part = jnp.concatenate([part, part], axis=1)
         part = part + jnp.where(t == 0, residual[source], 0.0)
         for k in range(8):
@@ -264,30 +264,29 @@
         out[y * 8 : y * 8 + 8, :] = total[:, 0:64].astype(BF16)
 
 
-def call(kernel, outs, *args, anywhere=(), scratch=()):
+def call(kernel, outs, *args, near=(0,), anywhere=(), scratch=()):
     specs = [
         pl.BlockSpec(memory_space=pl.ANY) if k in anywhere else pl.BlockSpec(memory_space=pltpu.VMEM)
         for k in range(len(args))
     ]
-    shapes = [jax.ShapeDtypeStruct(s, d) for s, d in outs]
+    args = [pltpu.with_memory_space_constraint(a, pltpu.VMEM) if k in near else a for k, a in enumerate(args)]
+    shapes = [pltpu.VMEM(s, d) for s, d in outs]
     found = pl.pallas_call(
         kernel,
         out_shape=shapes,
         in_specs=specs,
         out_specs=[pl.BlockSpec(memory_space=pltpu.VMEM) for _ in shapes],
         scratch_shapes=list(scratch),
-        name=kernel.__name__,
     )(*args)
     return found if len(shapes) > 1 else found[0]
 
 
-def around(value):
+def turned(value, d):
     n = lax.axis_size("y")
-    moved = [lax.ppermute(value, "y", [(k, (k + d) % n) for k in range(n)]) for d in range(1, n)]
-    return [value, *moved]
-
-
-def per_device(
+    return lax.ppermute(value, "y", [(k, (k + d) % n) for k in range(n)])
+
+
+def layer(
     stream,
     gain_in,
     w_query,
@@ -315,6 +314,7 @@
         w_key,
         w_value,
         w_forget.T,
+        near=(),
         anywhere=(6,),
         scratch=(pltpu.VMEM((16, 128), BF16), pltpu.SemaphoreType.DMA),
     )
@@ -322,16 +322,21 @@
     lines, stream_all, gain_all = call(
         spread_rows, [((16, 32, 128), BF16), ((2, 8, 128), F32), ((2, 8, 128), F32)], got
     )
-    lines, w_up, w_down = lax.optimization_barrier((lines, w_up, w_down))
+    lines, w_up, w_down = lax.optimization_barrier((lines, w_up, w_down.T))
     got = swap(lines, "z")
-    ups = around(w_up)
-    downs = around(w_down.T)
+    w0 = jnp.concatenate([w_up, w_down], axis=0)
+    w1 = turned(w0, 1)
+    w3 = turned(w0, 3)
     lines, own = call(finish_rows, [((4, 144, 128), BF16), ((8, 128), F32)], got, w_out.T)
+    lines, w1, w3 = lax.optimization_barrier((lines, w1, w3))
     w_all = swap(lines, "y")
     got = swap(attend(w_all[:, 0:16], keys_cache, values_cache, decay_cache, lengths, kv * 128), "y")
-    lines = call(merge_blocks, [((16, 24, 128), BF16)], got, own)
+    lines = call(merge_blocks, [((16, 24, 128), BF16)], got, own, near=(0, 1))
+    lines, w2 = lax.optimization_barrier((lines, w0))
     got = swap(lines, "z")
-    lines = call(project_out, [((8, 24, 128), F32)], got, w_all, gain_att.reshape(1, 256))
+    w2 = turned(w2, 2)
+    lines = call(project_out, [((8, 24, 128), F32)], got, w_all, gain_att.reshape(1, 256), near=(0, 1))
+    lines, w2 = lax.optimization_barrier((lines, w2))
     got = swap(lines, "tp")
     lines, residual = call(
         mix_up,
@@ -339,12 +344,16 @@
         got,
         stream_all,
         gain_all,
-        *ups,
+        w0,
+        w1,
+        w2,
+        w3,
+        near=tuple(range(7)),
         scratch=(pltpu.VMEM((4, 8, 128), F32),),
     )
     got = swap(lines, "z")
     got = swap(call(activate, [((16, 8, 128), BF16)], got), "z")
-    lines = call(mix_down, [((32, 8, 128), F32)], got, residual, *downs)
+    lines = call(mix_down, [((32, 8, 128), F32)], got, residual, w0, w1, w2, w3, near=tuple(range(6)))
     got = swap(lines, ("y", "tp"))
     return call(finish, [((32, 64), BF16)], got)
 
@@ -352,7 +361,7 @@
 def solution(mesh):
     split = Mesh(mesh.devices.reshape(16, 4, mesh.shape["tp"]), ("z", "y", "tp"))
     return jax.shard_map(
-        per_device,
+        layer,
         mesh=split,
         in_specs=(
             P(None, KV),

time: 169 us -> 154 us (0.911)
  blocking collectives: 33 us -> 77.8 us
  starting transfers between devices: 71.4 us -> 30.3 us
  Pallas kernels: 17.5 us -> 7.09 us
  waiting for transfers between devices: 36 us -> 28 us
    all_to_all x3 -> x6, blocking collectives: 33 us -> 77.8 us  [swap(): return lax.all_to_all(value, axis, split_axis=0, concat_axis=0, tiled=True)]
    all_to_all x6 -> x3, starting transfers between devices: 52.9 us -> 22.4 us  [swap(): return lax.all_to_all(value, axis, split_axis=0, concat_axis=0, tiled=True)]
    ppermute x6 -> x3, starting transfers between devices: 18.6 us -> 7.9 us  [turned(): return lax.ppermute(value, 'y', [(k, (k + d) % n) for k in range(n)])]
    pallas_call x9, Pallas kernels: 17.5 us -> 7.09 us  [call(): pl.pallas_call(kernel, out_shape=shapes, in_specs=specs, out_specs=[pl.Bl...]
    all_to_all x6 -> x3, waiting for transfers between devices: 36 us -> 28 us  [swap(): return lax.all_to_all(value, axis, split_axis=0, concat_axis=0, tiled=True)]
  transfers between devices with their start and end apart: 12 -> 6, of which waited for: 6 -> 3; matrix products, arithmetic and copies ran while one was open for 1% -> 0% of each run, Pallas kernels for 2% -> 2%
where the time goes in v2:
time: 154 us; the launch traced here: 153 us
  blocking collectives  77.8 us (51%)
  starting transfers between devices  30.3 us (20%)
  waiting for transfers between devices  28 us (18%)
  Pallas kernels  7.09 us (5%)
  matrix products  4.99 us (3%)
  local copies, waits for them, and re-layouts  4.37 us (3%)
    all_to_all x6, blocking collectives, swap(): return lax.all_to_all(value, axis, split_axis=0, concat_axis=0, tiled=True)  77.8 us
    all_to_all x3, waiting for transfers between devices, swap(): return lax.all_to_all(value, axis, split_axis=0, concat_axis=0, tiled=True)  28 us
    all_to_all x3, starting transfers between devices, swap(): return lax.all_to_all(value, axis, split_axis=0, concat_axis=0, tiled=True)  22.4 us
    ppermute x3, starting transfers between devices, turned(): return lax.ppermute(value, 'y', [(k, (k + d) % n) for k in range(n)])  7.9 us
    pallas_call x9, Pallas kernels, call(): pl.pallas_call(kernel, out_shape=shapes, in_specs=specs, out_specs=[pl.Bl...  7.09 us
  transfers between devices with their start and end apart: 6, of which 3 were waited for; matrix products, arithmetic and copies ran while one was open for 0% of the time, Pallas kernels for 2%

profile of v2, /device:TPU:1, one launch (start us, length us, event | category | flops | bytes accessed | tf_op | source)
XLA Modules:
  0.0 153.2 jit_solution(12842218576360979475)
XLA Ops:
  0.0 1.9 %shard_map.145 = f32[4,64,128]{2,1,0:T(8,128)S(1)} custom-call(bf16[32,64]{1,0:T(8,128)(2,1)} %stream.1, bf16[1,64]{1,0:T(2,128)(2,1)} %bitcast.39, bf16[1,64]{1,0:T(2,128)(2,1)} %bitcast.40, bf16[64,256]{1,0:T(8,128)(2,1)} %w_query.1, bf16[64,256]{1,0:T(8,128)(2,1)} %w_key.1, bf16[64,256]{1,0:T(8,128)(2,1)} %w_value.1, bf16[16,4096]{1,0:T(8,128)(2,1)} %bitcast.35), custom_call_target="tpu_custom_call" | custom-call | tf_op jit(solution)/shard_map/pallas_call | solution.py:274
  1.9 9.6 %all_to_all.45.got = f32[4,64,128]{2,1,0:T(8,128)S(1)} all-to-all(f32[4,64,128]{2,1,0:T(8,128)S(1)} %shard_map.145), channel_id=1, replica_groups=mesh['z'=16,'y'=4,'tp'=8] {'y'}, dimensions={0} | all-to-all | bytes 262144 | tf_op jit(solution)/shard_map/all_to_all | solution.py:21
  11.5 0.7 shard_map.146
  12.2 1.0 constant_dynamic-update-slice_fusion.1
  13.2 1.0 constant_dynamic-update-slice_fusion.w0
  14.2 2.8 %collective-permute-start.1 = (bf16[128,2048]{1,0:T(8,128)(2,1)S(1)}, bf16[128,2048]{1,0:T(8,128)(2,1)S(1)}, u32[]{:S(2)}, u32[]{:S(2)}) collective-permute-start(bf16[128,2048]{1,0:T(8,128)(2,1)S(1)} %constant_dynamic-update-slice_fusion.w0), channel_id=1, source_target_pairs={{0,24},{8,0},{16,8},{24,16},{1,25},{9,1},{17,9},{25,17},{2,26},{10... | collective-permute-start | bytes 1572872 | tf_op jit(solution)/shard_map/ppermute | solution.py:286
  17.0 2.5 %collective-permute-start = (bf16[128,2048]{1,0:T(8,128)(2,1)S(1)}, bf16[128,2048]{1,0:T(8,128)(2,1)S(1)}, u32[]{:S(2)}, u32[]{:S(2)}) collective-permute-start(bf16[128,2048]{1,0:T(8,128)(2,1)S(1)} %constant_dynamic-update-slice_fusion.w0), channel_id=1, source_target_pairs={{0,8},{8,16},{16,24},{24,0},{1,9},{9,17},{17,25},{25,1},{2,10},{10... | collective-permute-start | bytes 1572872 | tf_op jit(solution)/shard_map/ppermute | solution.py:286
  19.5 14.9 %all-to-all-start.1 = ((bf16[16,32,128]{2,1,0:T(8,128)(2,1)}), bf16[16,32,128]{2,1,0:T(8,128)(2,1)S(1)}, u32[]{:S(2)}, u32[]{:S(2)}) async-start(bf16[16,32,128]{2,1,0:T(8,128)(2,1)} %get-tuple-element.23), calls=%async_computation.1 | async-start | bytes 262144 | tf_op jit(solution)/shard_map/all_to_all | solution.py:21
  34.5 11.9 %all-to-all-done.1.got = bf16[16,32,128]{2,1,0:T(8,128)(2,1)S(1)} async-done(((bf16[16,32,128]{2,1,0:T(8,128)(2,1)}), bf16[16,32,128]{2,1,0:T(8,128)(2,1)S(1)}, u32[]{:S(2)}, u32[]{:S(2)}) %all-to-all-start.1) | async-done | bytes 131104 | tf_op jit(solution)/shard_map/all_to_all | solution.py:21
  46.4 1.7 %shard_map.147 = (bf16[4,144,128]{2,1,0:T(8,128)(2,1)}, f32[8,128]{1,0:T(8,128)S(1)}) custom-call(bf16[16,32,128]{2,1,0:T(8,128)(2,1)S(1)} %all-to-all-done.1.got, bf16[64,256]{1,0:T(8,128)(2,1)} %bitcast.38), custom_call_target="tpu_custom_call" | custom-call | tf_op jit(solution)/shard_map/pallas_call | solution.py:274
  48.0 3.4 %all-to-all-start.2 = ((bf16[4,144,128]{2,1,0:T(8,128)(2,1)}), bf16[4,144,128]{2,1,0:T(8,128)(2,1)S(1)}, u32[]{:S(2)}, u32[]{:S(2)}) async-start(bf16[4,144,128]{2,1,0:T(8,128)(2,1)} %get-tuple-element.27), calls=%async_computation.2 | async-start | bytes 294912 | tf_op jit(solution)/shard_map/all_to_all | solution.py:21
  51.4 4.9 %all-to-all-done.2.w_all = bf16[4,144,128]{2,1,0:T(8,128)(2,1)S(1)} async-done(((bf16[4,144,128]{2,1,0:T(8,128)(2,1)}), bf16[4,144,128]{2,1,0:T(8,128)(2,1)S(1)}, u32[]{:S(2)}, u32[]{:S(2)}) %all-to-all-start.2) | async-done | bytes 147488 | tf_op jit(solution)/shard_map/all_to_all | solution.py:21
  56.3 2.8 %fusion.2 = f32[32,2,1,128]{3,2,1,0:T(1,128)S(1)} fusion(bf16[32,2,128,128]{3,2,1,0:T(8,128)(2,1)} %param.21, bf16[32,2,128,1]{2,0,1,3:T(8,128)(2,1)S(1)} %copy_bitcast_fusion.1), kind=kOutput, calls=%fused_computation.4 | convolution fusion | flops 2097152 | bytes 2146304 | tf_op jit(solution)/shard_map/shd,shpd->shp/dot_general | solution.py:133
  59.1 0.1 fusion.5
  59.2 0.2 convert_bitcast_fusion
  59.6 2.2 %fusion = f32[32,2,1,128]{3,2,1,0:T(1,128)S(1)} fusion(bf16[32,2,128,128]{3,2,1,0:T(8,128)(2,1)} %param.22, bf16[32,2,128,1]{2,1,0,3:T(2,128)(2,1)S(1)} %get-tuple-element.39), kind=kOutput, calls=%fused_computation.2 | convolution fusion | flops 2097152 | bytes 2146304 | tf_op jit(solution)/shard_map/shp,shpd->shd/dot_general | solution.py:140
  62.0 6.8 %all_to_all.46.got = f32[4,32,128]{2,1,0:T(8,128)S(1)} all-to-all(f32[4,32,128]{2,1,0:T(8,128)S(1)} %bitcast.33), channel_id=1, replica_groups=mesh['z'=16,'y'=4,'tp'=8] {'y'}, dimensions={0} | all-to-all | bytes 131072 | tf_op jit(solution)/shard_map/all_to_all | solution.py:21
  68.8 0.8 shard_map.148
  69.6 2.6 %collective-permute-start.2 = (bf16[128,2048]{1,0:T(8,128)(2,1)S(1)}, bf16[128,2048]{1,0:T(8,128)(2,1)S(1)}, u32[]{:S(2)}, u32[]{:S(2)}) collective-permute-start(bf16[128,2048]{1,0:T(8,128)(2,1)S(1)} %constant_dynamic-update-slice_fusion.w0), channel_id=1, source_target_pairs={{0,16},{8,24},{16,0},{24,8},{1,17},{9,25},{17,1},{25,9},{2,18},{10... | collective-permute-start | bytes 1572872 | tf_op jit(solution)/shard_map/ppermute | solution.py:286
  72.3 4.1 %all-to-all-start.4 = ((bf16[16,24,128]{2,1,0:T(8,128)(2,1)}), bf16[16,24,128]{2,1,0:T(8,128)(2,1)S(1)}, u32[]{:S(2)}, u32[]{:S(2)}) async-start(bf16[16,24,128]{2,1,0:T(8,128)(2,1)} %shard_map.148), calls=%async_computation.4 | async-start | bytes 196608 | tf_op jit(solution)/shard_map/all_to_all | solution.py:21
  76.3 0.6 reshape.63.gain_att
  76.9 11.3 %all-to-all-done.4.got = bf16[16,24,128]{2,1,0:T(8,128)(2,1)S(1)} async-done(((bf16[16,24,128]{2,1,0:T(8,128)(2,1)}), bf16[16,24,128]{2,1,0:T(8,128)(2,1)S(1)}, u32[]{:S(2)}, u32[]{:S(2)}) %all-to-all-start.4) | async-done | bytes 98336 | tf_op jit(solution)/shard_map/all_to_all | solution.py:21
  88.2 1.0 shard_map.149
  89.2 17.1 %all_to_all.47.got = f32[8,24,128]{2,1,0:T(8,128)S(1)} all-to-all(f32[8,24,128]{2,1,0:T(8,128)S(1)} %shard_map.149), channel_id=1, replica_groups=mesh['z'=16,'y'=4,'tp'=8] {'tp'}, dimensions={0} | all-to-all | bytes 196608 | tf_op jit(solution)/shard_map/all_to_all | solution.py:21
  106.3 0.4 shard_map.150
  106.7 14.6 %all_to_all.48.got = bf16[16,16,128]{2,1,0:T(8,128)(2,1)S(1)} all-to-all(bf16[16,16,128]{2,1,0:T(8,128)(2,1)S(1)} %get-tuple-element.37), channel_id=1, replica_groups=mesh['z'=16,'y'=4,'tp'=8] {'z'}, dimensions={0} | all-to-all | bytes 131072 | tf_op jit(solution)/shard_map/all_to_all | solution.py:21
  121.3 0.2 shard_map.151
  121.5 14.3 %all_to_all.49.got = bf16[16,8,128]{2,1,0:T(8,128)(2,1)S(1)} all-to-all(bf16[16,8,128]{2,1,0:T(8,128)(2,1)S(1)} %shard_map.151), channel_id=1, replica_groups=mesh['z'=16,'y'=4,'tp'=8] {'z'}, dimensions={0} | all-to-all | bytes 65536 | tf_op jit(solution)/shard_map/all_to_all | solution.py:21
  135.8 1.0 copy-done.1
  136.9 0.4 shard_map.152
  137.3 15.3 %all_to_all.50.got = f32[32,8,128]{2,1,0:T(8,128)S(1)} all-to-all(f32[32,8,128]{2,1,0:T(8,128)S(1)} %shard_map.152), channel_id=1, replica_groups=mesh['z'=16,'y'=4,'tp'=8] {'y','tp'}, dimensions={0} | all-to-all | bytes 262144 | tf_op jit(solution)/shard_map/all_to_all | solution.py:21
  152.6 0.6 copy.40
  (23 shorter events, 0.4 us)
Async XLA Ops:
  0.0 34.4 %copy-start.3 = (s32[32]{0:T(128)S(1)}, s32[32]{0:T(128)}, u32[]{:S(2)}) copy-start(s32[32]{0:T(128)} %param.24) | copy-start | bytes 388
  11.5 47.6 %copy-start.2 = (f32[32,2,128]{2,1,0:T(2,128)S(1)}, f32[32,2,128]{2,1,0:T(2,128)}, u32[]{:S(2)}) copy-start(f32[32,2,128]{2,1,0:T(2,128)} %param.23) | copy-start | bytes 98308
  14.2 33.9 %collective-permute-start.1 = (bf16[128,2048]{1,0:T(8,128)(2,1)S(1)}, bf16[128,2048]{1,0:T(8,128)(2,1)S(1)}, u32[]{:S(2)}, u32[]{:S(2)}) collective-permute-start(bf16[128,2048]{1,0:T(8,128)(2,1)S(1)} %constant_dynamic-update-slice_fusion.w0), channel_id=1, source_target_pairs={{0,24},{8,0},{16,8},{24,16},{1,25},{9,1},{17,9},{25,17},{2,26},{10... | collective-permute-start | bytes 1572872 | tf_op jit(solution)/shard_map/ppermute | solution.py:286
  17.0 31.1 %collective-permute-start = (bf16[128,2048]{1,0:T(8,128)(2,1)S(1)}, bf16[128,2048]{1,0:T(8,128)(2,1)S(1)}, u32[]{:S(2)}, u32[]{:S(2)}) collective-permute-start(bf16[128,2048]{1,0:T(8,128)(2,1)S(1)} %constant_dynamic-update-slice_fusion.w0), channel_id=1, source_target_pairs={{0,8},{8,16},{16,24},{24,0},{1,9},{9,17},{17,25},{25,1},{2,10},{10... | collective-permute-start | bytes 1572872 | tf_op jit(solution)/shard_map/ppermute | solution.py:286
  19.5 26.9 %all-to-all-start.1 = ((bf16[16,32,128]{2,1,0:T(8,128)(2,1)}), bf16[16,32,128]{2,1,0:T(8,128)(2,1)S(1)}, u32[]{:S(2)}, u32[]{:S(2)}) async-start(bf16[16,32,128]{2,1,0:T(8,128)(2,1)} %get-tuple-element.23), calls=%async_computation.1 | async-start | bytes 262144 | tf_op jit(solution)/shard_map/all_to_all | solution.py:21
  48.0 58.3 %copy-start = (bf16[128,2048]{1,0:T(8,128)(2,1)}, bf16[128,2048]{1,0:T(8,128)(2,1)S(1)}, u32[]{:S(2)}) copy-start(bf16[128,2048]{1,0:T(8,128)(2,1)S(1)} %collective-permute-done.w1) | copy-start | bytes 1572868
  48.0 8.3 %all-to-all-start.2 = ((bf16[4,144,128]{2,1,0:T(8,128)(2,1)}), bf16[4,144,128]{2,1,0:T(8,128)(2,1)S(1)}, u32[]{:S(2)}, u32[]{:S(2)}) async-start(bf16[4,144,128]{2,1,0:T(8,128)(2,1)} %get-tuple-element.27), calls=%async_computation.2 | async-start | bytes 294912 | tf_op jit(solution)/shard_map/all_to_all | solution.py:21
  59.1 17.2 %copy-start.4 = (bf16[256]{0:T(256)(128)(2,1)S(1)}, bf16[256]{0:T(256)(128)(2,1)}, u32[]{:S(2)}) copy-start(bf16[256]{0:T(256)(128)(2,1)} %param.25) | copy-start | bytes 1540
  69.6 19.6 %collective-permute-start.2 = (bf16[128,2048]{1,0:T(8,128)(2,1)S(1)}, bf16[128,2048]{1,0:T(8,128)(2,1)S(1)}, u32[]{:S(2)}, u32[]{:S(2)}) collective-permute-start(bf16[128,2048]{1,0:T(8,128)(2,1)S(1)} %constant_dynamic-update-slice_fusion.w0), channel_id=1, source_target_pairs={{0,16},{8,24},{16,0},{24,8},{1,17},{9,25},{17,1},{25,9},{2,18},{10... | collective-permute-start | bytes 1572872 | tf_op jit(solution)/shard_map/ppermute | solution.py:286
  72.3 15.9 %all-to-all-start.4 = ((bf16[16,24,128]{2,1,0:T(8,128)(2,1)}), bf16[16,24,128]{2,1,0:T(8,128)(2,1)S(1)}, u32[]{:S(2)}, u32[]{:S(2)}) async-start(bf16[16,24,128]{2,1,0:T(8,128)(2,1)} %shard_map.148), calls=%async_computation.4 | async-start | bytes 196608 | tf_op jit(solution)/shard_map/all_to_all | solution.py:21
  135.8 1.0 copy-start.1

commit v3 on v2

--- a/solution.py
+++ b/solution.py
@@ -13,6 +13,7 @@
 masked_score = -1e30
 F32 = jnp.float32
 BF16 = jnp.bfloat16
+LIMIT = 8 * 1024 * 1024
 WIDTH = 4096
 HEADS_WIDTH = 2048
 
@@ -128,20 +129,42 @@
         out[y, 80:144, :] = w[:, 128:256]
 
 
-def attend(q, keys, values, decay, lengths, first):
-    q = q.reshape(4, 2, 8, 128).swapaxes(1, 2).reshape(32, 2, 128)
-    s = jnp.einsum("shd,shpd->shp", q, keys, preferred_element_type=F32)
-    s = s * (1.0 / math.sqrt(128)) + decay
-    live = (first + lax.iota(jnp.int32, 128)[None, :] < lengths[:, None])[:, None, :]
-    s = jnp.where(live, s, masked_score)
-    peak = jnp.max(s, axis=2, keepdims=True)
-    probs = jnp.where(live, jnp.exp(s - peak), 0.0)
-    total = jnp.sum(probs, axis=2, keepdims=True)
-    out = jnp.einsum("shp,shpd->shd", probs.astype(BF16), values, preferred_element_type=F32)
-    lane = lax.broadcasted_iota(jnp.int32, (32, 2, 128), 2)
-    extra = jnp.where(lane == 0, peak, total)
-    both = jnp.stack([out, extra]).reshape(2, 4, 8, 2, 128)
-    return both.transpose(1, 0, 3, 2, 4).reshape(4, 32, 128)
+def attend(w_all, keys, values_far, decay, lengths, out, values, sems):
+    copies = []
+    for y in range(4):
+        part = pl.ds(y * 8, 8)
+        copies.append(pltpu.make_async_copy(values_far.at[part], values.at[part], sems.at[y]))
+        copies[y].start()
+    first = (lax.axis_index("z") * 4 + lax.axis_index("y")) * 128
+    place = lanes(8) + first
+    row = lax.broadcasted_iota(jnp.int32, (8, 128), 0)
+    for y in range(4):
+        q = w_all[y, 0:16, :]
+        every = dot_nt(q, keys[y * 8 : y * 8 + 8].reshape(2048, 128))
+        length = jnp.zeros((8, 128), jnp.int32)
+        for b in range(8):
+            length = jnp.where(row == b, lengths[y * 8 + b], length)
+        live = place < length
+        probs = []
+        for h in range(2):
+            s = jnp.zeros((8, 128), F32)
+            for b in range(8):
+                c = (b * 2 + h) * 128
+                s = jnp.where(row == b, every[h * 8 : h * 8 + 8, c : c + 128], s)
+            s = s * (1.0 / math.sqrt(128)) + decay[y * 8 : y * 8 + 8, h, :]
+            s = jnp.where(live, s, masked_score)
+            peak = jnp.max(s, axis=1, keepdims=True)
+            p = jnp.where(live, jnp.exp(s - peak), 0.0)
+            out[y, 16 + h * 8 : 24 + h * 8, :] = columns([peak, jnp.sum(p, axis=1, keepdims=True)])
+            probs.append(p)
+        wide = []
+        for b in range(8):
+            for h in range(2):
+                own = jnp.where(row == b, probs[h], 0.0)
+                none = jnp.zeros((8, 128), F32)
+                wide.append(jnp.concatenate([own, none] if h == 0 else [none, own], axis=0).astype(BF16))
+        copies[y].wait()
+        out[y, 0:16, :] = dot(jnp.concatenate(wide, axis=1), values[y * 8 : y * 8 + 8].reshape(2048, 128))
 
 
 def merge_blocks(got, own, out):
@@ -205,7 +228,7 @@
         out[k, 16:24, :] = extra
 
 
-def mix_up(got, stream_all, gain_all, w0, w1, w2, w3, out, residual_out, halves):
+def mix_up(got, stream_all, gain_all, near, far, out, residual_out, halves):
     y = lax.axis_index("y")
     total = got[0]
     for k in range(1, 8):
@@ -216,14 +239,12 @@
         residual = high(stream_all[k] + scale * total[k * 8 : k * 8 + 8])
         squares = squares + jnp.sum(residual * residual, axis=1, keepdims=True)
         mixer_in = high(residual * gain_all[k])
-        halves[2 * k] = mixer_in
-        halves[2 * k + 1] = pltpu.roll(mixer_in, 64, 1)
+        halves[k] = mixer_in
+        halves[2 + k] = pltpu.roll(mixer_in, 64, 1)
         residual_out[2 * k] = residual
         residual_out[2 * k + 1] = pltpu.roll(residual, 64, 1)
-    up = jnp.zeros((8, 2048), F32)
-    for d, w in enumerate((w0, w1, w2, w3)):
-        lhs = halves[(y + 4 - d) % 4][:, 0:64].astype(BF16)
-        up = up + dot(lhs, w[0:64, :])
+    up = dot(halves[y // 2 + 2 * (y % 2)].astype(BF16), near[...])
+    up = up + dot(halves[1 - y // 2 + 2 * (1 - y % 2)].astype(BF16), far[...])
     one = high(squares)
     two = high(squares - one)
     extra = columns([one, two, squares - one - two])
@@ -243,17 +264,17 @@
         out[k] = hidden
 
 
-def mix_down(got, residual, w0, w1, w2, w3, out):
+def mix_down(got, residual, near, far, out):
     y = lax.axis_index("y")
     t = lax.axis_index("tp")
     hidden = jnp.concatenate([got[k] for k in range(16)], axis=1)
-    for d, w in enumerate((w0, w1, w2, w3)):
-        source = (y + 4 - d) % 4
-        part = dot_nt(hidden, w[64:128, :])
-        part = jnp.concatenate([part, part], axis=1)
-        part = part + jnp.where(t == 0, residual[source], 0.0)
-        for k in range(8):
-            out[source * 8 + k] = part
+    places = ((y, y + 1 - 2 * (y % 2)), (3 - y, (y + 2) % 4))
+    for w, targets in zip((near, far), places):
+        both = dot_nt(hidden, w[...])
+        for target, part in zip(targets, (both, pltpu.roll(both, 64, 1))):
+            part = part + jnp.where(t == 0, residual[target], 0.0)
+            for k in range(8):
+                out[target * 8 + k] = part
 
 
 def finish(got, out):
@@ -264,12 +285,15 @@
         out[y * 8 : y * 8 + 8, :] = total[:, 0:64].astype(BF16)
 
 
-def call(kernel, outs, *args, near=(0,), anywhere=(), scratch=()):
-    specs = [
-        pl.BlockSpec(memory_space=pl.ANY) if k in anywhere else pl.BlockSpec(memory_space=pltpu.VMEM)
-        for k in range(len(args))
-    ]
-    args = [pltpu.with_memory_space_constraint(a, pltpu.VMEM) if k in near else a for k, a in enumerate(args)]
+def call(kernel, outs, *args, near=(0,), anywhere=(), scalars=(), scratch=()):
+    specs = []
+    placed = []
+    for k, a in enumerate(args):
+        space = pl.ANY if k in anywhere else pltpu.SMEM if k in scalars else pltpu.VMEM
+        specs.append(pl.BlockSpec(memory_space=space))
+        if k not in scalars:
+            a = pltpu.with_memory_space_constraint(a, pltpu.VMEM if k in near else pltpu.HBM)
+        placed.append(a)
     shapes = [pltpu.VMEM(s, d) for s, d in outs]
     found = pl.pallas_call(
         kernel,
@@ -277,13 +301,26 @@
         in_specs=specs,
         out_specs=[pl.BlockSpec(memory_space=pltpu.VMEM) for _ in shapes],
         scratch_shapes=list(scratch),
-    )(*args)
+        compiler_params=pltpu.CompilerParams(vmem_limit_bytes=LIMIT),
+    )(*placed)
     return found if len(shapes) > 1 else found[0]
 
 
-def turned(value, d):
-    n = lax.axis_size("y")
-    return lax.ppermute(value, "y", [(k, (k + d) % n) for k in range(n)])
+def fetch(keys, w_out, decay, keys_out, w_out_out, decay_out, sems):
+    pairs = ((keys, keys_out), (w_out, w_out_out), (decay, decay_out))
+    copies = [pltpu.make_async_copy(a, b, sems.at[k]) for k, (a, b) in enumerate(pairs)]
+    for copy in copies:
+        copy.start()
+    for copy in copies:
+        copy.wait()
+
+
+def beside(value):
+    return lax.ppermute(value, "y", [(0, 1), (1, 0), (2, 3), (3, 2)])
+
+
+def across(value):
+    return lax.ppermute(value, "y", [(0, 3), (3, 0), (1, 2), (2, 1)])
 
 
 def layer(
@@ -303,7 +340,6 @@
     w_up,
     w_down,
 ):
-    kv = lax.axis_index(KV)
     lines = call(
         project,
         [((4, 64, 128), F32)],
@@ -322,21 +358,43 @@
     lines, stream_all, gain_all = call(
         spread_rows, [((16, 32, 128), BF16), ((2, 8, 128), F32), ((2, 8, 128), F32)], got
     )
-    lines, w_up, w_down = lax.optimization_barrier((lines, w_up, w_down.T))
+    lines, w_up, keys_cache = lax.optimization_barrier((lines, w_up, keys_cache))
     got = swap(lines, "z")
-    w0 = jnp.concatenate([w_up, w_down], axis=0)
-    w1 = turned(w0, 1)
-    w3 = turned(w0, 3)
-    lines, own = call(finish_rows, [((4, 144, 128), BF16), ((8, 128), F32)], got, w_out.T)
-    lines, w1, w3 = lax.optimization_barrier((lines, w1, w3))
+    keys, w_out, decay = call(
+        fetch,
+        [(keys_cache.shape, BF16), ((64, 256), BF16), (decay_cache.shape, F32)],
+        keys_cache,
+        w_out.T,
+        decay_cache,
+        near=(),
+        anywhere=(0, 1, 2),
+        scratch=(pltpu.SemaphoreType.DMA((3,)),),
+    )
+    other = beside(w_up)
+    lines, own = call(finish_rows, [((4, 144, 128), BF16), ((8, 128), F32)], got, w_out, near=(0, 1))
+    lines, other = lax.optimization_barrier((lines, other))
     w_all = swap(lines, "y")
-    got = swap(attend(w_all[:, 0:16], keys_cache, values_cache, decay_cache, lengths, kv * 128), "y")
+    lines = call(
+        attend,
+        [((4, 32, 128), F32)],
+        w_all,
+        keys,
+        values_cache,
+        decay,
+        lengths,
+        near=(0, 1, 3),
+        anywhere=(2,),
+        scalars=(4,),
+        scratch=(pltpu.VMEM((32, 2, 128, 128), BF16), pltpu.SemaphoreType.DMA((4,))),
+    )
+    got = swap(lines, "y")
     lines = call(merge_blocks, [((16, 24, 128), BF16)], got, own, near=(0, 1))
-    lines, w2 = lax.optimization_barrier((lines, w0))
+    up_near = jnp.concatenate([w_up, other], axis=0)
+    lines, up_near, w_down = lax.optimization_barrier((lines, up_near, w_down.T))
     got = swap(lines, "z")
-    w2 = turned(w2, 2)
+    up_far = across(up_near)
+    other = beside(w_down)
     lines = call(project_out, [((8, 24, 128), F32)], got, w_all, gain_att.reshape(1, 256), near=(0, 1))
-    lines, w2 = lax.optimization_barrier((lines, w2))
     got = swap(lines, "tp")
     lines, residual = call(
         mix_up,
@@ -344,16 +402,17 @@
         got,
         stream_all,
         gain_all,
-        w0,
-        w1,
-        w2,
-        w3,
-        near=tuple(range(7)),
+        up_near,
+        up_far,
+        near=tuple(range(5)),
         scratch=(pltpu.VMEM((4, 8, 128), F32),),
     )
+    down_near = jnp.concatenate([w_down, other], axis=0)
+    lines, down_near = lax.optimization_barrier((lines, down_near))
     got = swap(lines, "z")
+    down_far = across(down_near)
     got = swap(call(activate, [((16, 8, 128), BF16)], got), "z")
-    lines = call(mix_down, [((32, 8, 128), F32)], got, residual, w0, w1, w2, w3, near=tuple(range(6)))
+    lines = call(mix_down, [((32, 8, 128), F32)], got, residual, down_near, down_far, near=tuple(range(4)))
     got = swap(lines, ("y", "tp"))
     return call(finish, [((32, 64), BF16)], got)
 

time: 154 us -> 147 us (0.955)
  starting transfers between devices: 30.3 us -> 46.1 us
  blocking collectives: 77.8 us -> 62.9 us
  matrix products: 4.99 us -> 0 us
  Pallas kernels: 7.09 us -> 12 us
  waiting for transfers between devices: 28 us -> 24.1 us
  local copies, waits for them, and re-layouts: 4.37 us -> 1.18 us
    all_to_all x6 -> x5, blocking collectives: 77.8 us -> 62.9 us  [swap(): return lax.all_to_all(value, axis, split_axis=0, concat_axis=0, tiled=True)]
    all_to_all x3 -> x4, starting transfers between devices: 22.4 us -> 36.4 us  [swap(): return lax.all_to_all(value, axis, split_axis=0, concat_axis=0, tiled=True)]
    dot_general x2 -> x0, matrix products: 4.99 us -> none  [the longest x1 2.75 us: attend(): s = jnp.einsum('shd,shpd->shp', q, keys, preferred_element_type=F32)]
    pallas_call x9 -> x11, Pallas kernels: 7.09 us -> 12 us  [call(): pl.pallas_call(kernel, out_shape=shapes, in_specs=specs, out_specs=[pl.Bl...]
    all_to_all x3 -> x4, waiting for transfers between devices: 28 us -> 24.1 us  [swap(): return lax.all_to_all(value, axis, split_axis=0, concat_axis=0, tiled=True)]
    unnamed x12 -> x9, local copies, waits for them, and re-layouts: 2.62 us -> 0.62 us
    ppermute x3 -> x4, starting transfers between devices: 7.9 us -> 9.7 us  [the longest x2 5.59 us: across(): return lax.ppermute(value, 'y', [(0, 3), (3, 0), (1, 2), (2, 1)])]
  transfers between devices with their start and end apart: 6 -> 8, of which waited for: 3 -> 4; matrix products, arithmetic and copies ran while one was open for 0% -> 0% of each run, Pallas kernels for 2% -> 3%
where the time goes in v3:
time: 147 us
  blocking collectives  62.9 us (43%)
  starting transfers between devices  46.1 us (31%)
  waiting for transfers between devices  24.1 us (16%)
  Pallas kernels  12 us (8%)
    all_to_all x5, blocking collectives, swap(): return lax.all_to_all(value, axis, split_axis=0, concat_axis=0, tiled=True)  62.9 us
    all_to_all x4, starting transfers between devices, swap(): return lax.all_to_all(value, axis, split_axis=0, concat_axis=0, tiled=True)  36.4 us
    all_to_all x4, waiting for transfers between devices, swap(): return lax.all_to_all(value, axis, split_axis=0, concat_axis=0, tiled=True)  24.1 us
    pallas_call x11, Pallas kernels, call(): pl.pallas_call(kernel, out_shape=shapes, in_specs=specs, out_specs=[pl.Bl...  12 us
    ppermute x2, starting transfers between devices, across(): return lax.ppermute(value, 'y', [(0, 3), (3, 0), (1, 2), (2, 1)])  5.59 us
    ppermute x2, starting transfers between devices, beside(): return lax.ppermute(value, 'y', [(0, 1), (1, 0), (2, 3), (3, 2)])  4.12 us
  transfers between devices with their start and end apart: 8, of which 4 were waited for; matrix products, arithmetic and copies ran while one was open for 0% of the time, Pallas kernels for 3%

profile of v3, /device:TPU:1, one launch (start us, length us, event | category | flops | bytes accessed | tf_op | source)
XLA Modules:
  0.0 146.5 jit_solution(17622803225654242574)
XLA Ops:
  0.0 1.9 %shard_map.145 = f32[4,64,128]{2,1,0:T(8,128)S(1)} custom-call(bf16[32,64]{1,0:T(8,128)(2,1)} %stream.1, bf16[1,64]{1,0:T(2,128)(2,1)} %bitcast.9, bf16[1,64]{1,0:T(2,128)(2,1)} %bitcast.10, bf16[64,256]{1,0:T(8,128)(2,1)} %w_query.1, bf16[64,256]{1,0:T(8,128)(2,1)} %w_key.1, bf16[64,256]{1,0:T(8,128)(2,1)} %w_value.1, bf16[16,4096]{1,0:T(8,128)(2,1)} %bitcast.7), custom_call_target="tpu_custom_call" | custom-call | tf_op jit(solution)/shard_map/pallas_call | solution.py:298
  1.9 9.6 %all_to_all.45.got = f32[4,64,128]{2,1,0:T(8,128)S(1)} all-to-all(f32[4,64,128]{2,1,0:T(8,128)S(1)} %shard_map.145), channel_id=1, replica_groups=mesh['z'=16,'y'=4,'tp'=8] {'y'}, dimensions={0} | all-to-all | bytes 262144 | tf_op jit(solution)/shard_map/all_to_all | solution.py:22
  11.5 0.7 shard_map.146
  12.2 14.9 %all-to-all-start.1 = ((bf16[16,32,128]{2,1,0:T(8,128)(2,1)}), bf16[16,32,128]{2,1,0:T(8,128)(2,1)S(1)}, u32[]{:S(2)}, u32[]{:S(2)}) async-start(bf16[16,32,128]{2,1,0:T(8,128)(2,1)} %get-tuple-element.26), calls=%async_computation.1 | async-start | bytes 262144 | tf_op jit(solution)/shard_map/all_to_all | solution.py:22
  27.2 2.2 %collective-permute-start = (bf16[64,2048]{1,0:T(8,128)(2,1)}, bf16[64,2048]{1,0:T(8,128)(2,1)S(1)}, u32[]{:S(2)}, u32[]{:S(2)}) collective-permute-start(bf16[64,2048]{1,0:T(8,128)(2,1)} %param.28), channel_id=1, source_target_pairs={{0,8},{8,0},{16,24},{24,16},{1,9},{9,1},{17,25},{25,17},{2,10},{10... | collective-permute-start | bytes 786440 | tf_op jit(solution)/shard_map/ppermute | solution.py:319
  29.4 1.6 %shard_map.147 = (bf16[32,2,128,128]{3,2,1,0:T(8,128)(2,1)S(1)}, bf16[64,256]{1,0:T(8,128)(2,1)S(1)}, f32[32,2,128]{2,1,0:T(2,128)S(1)}) custom-call(bf16[32,2,128,128]{3,2,1,0:T(8,128)(2,1)} %keys, bf16[64,256]{1,0:T(8,128)(2,1)} %bitcast.8, f32[32,2,128]{2,1,0:T(2,128)} %decay.1), custom_call_target="tpu_custom_call" | custom-call | tf_op jit(solution)/shard_map/pallas_call | solution.py:298
  31.0 8.1 %all-to-all-done.1.got = bf16[16,32,128]{2,1,0:T(8,128)(2,1)S(1)} async-done(((bf16[16,32,128]{2,1,0:T(8,128)(2,1)}), bf16[16,32,128]{2,1,0:T(8,128)(2,1)S(1)}, u32[]{:S(2)}, u32[]{:S(2)}) %all-to-all-start.1) | async-done | bytes 131104 | tf_op jit(solution)/shard_map/all_to_all | solution.py:22
  39.1 0.4 shard_map.148
  39.5 0.0 collective-permute-done
  39.5 7.3 %all_to_all.46.w_all = bf16[4,144,128]{2,1,0:T(8,128)(2,1)S(1)} all-to-all(bf16[4,144,128]{2,1,0:T(8,128)(2,1)S(1)} %get-tuple-element.31), channel_id=1, replica_groups=mesh['z'=16,'y'=4,'tp'=8] {'y'}, dimensions={0} | all-to-all | bytes 294912 | tf_op jit(solution)/shard_map/all_to_all | solution.py:22
  46.8 4.0 %shard_map.149 = f32[4,32,128]{2,1,0:T(8,128)} custom-call(bf16[4,144,128]{2,1,0:T(8,128)(2,1)S(1)} %all_to_all.46.w_all, bf16[32,2,128,128]{3,2,1,0:T(8,128)(2,1)S(1)} %get-tuple-element.32.keys, bf16[32,2,128,128]{3,2,1,0:T(8,128)(2,1)} %values_far.1, f32[32,2,128]{2,1,0:T(2,128)S(1)} %get-tuple-element.33.decay, s32[32]{0:T(128)S(1)} %copy-done), custom_call_target="tpu_custom_call" | custom-call | tf_op jit(solution)/shard_map/pallas_call | solution.py:298
  50.8 3.3 %all-to-all-start.3 = ((f32[4,32,128]{2,1,0:T(8,128)}), f32[4,32,128]{2,1,0:T(8,128)S(1)}, u32[]{:S(2)}, u32[]{:S(2)}) async-start(f32[4,32,128]{2,1,0:T(8,128)} %shard_map.149), calls=%async_computation.3 | async-start | bytes 131072 | tf_op jit(solution)/shard_map/all_to_all | solution.py:22
  54.1 4.4 %all-to-all-done.3.got = f32[4,32,128]{2,1,0:T(8,128)S(1)} async-done(((f32[4,32,128]{2,1,0:T(8,128)}), f32[4,32,128]{2,1,0:T(8,128)S(1)}, u32[]{:S(2)}, u32[]{:S(2)}) %all-to-all-start.3) | async-done | bytes 65568 | tf_op jit(solution)/shard_map/all_to_all | solution.py:22
  58.5 0.8 shard_map.150
  59.3 6.5 %all-to-all-start.4 = ((bf16[16,24,128]{2,1,0:T(8,128)(2,1)}), bf16[16,24,128]{2,1,0:T(8,128)(2,1)S(1)}, u32[]{:S(2)}, u32[]{:S(2)}) async-start(bf16[16,24,128]{2,1,0:T(8,128)(2,1)} %shard_map.150), calls=%async_computation.4 | async-start | bytes 196608 | tf_op jit(solution)/shard_map/all_to_all | solution.py:22
  65.8 2.8 %collective-permute-start.1 = (bf16[128,2048]{1,0:T(8,128)(2,1)S(1)}, bf16[128,2048]{1,0:T(8,128)(2,1)S(1)}, u32[]{:S(2)}, u32[]{:S(2)}) collective-permute-start(bf16[128,2048]{1,0:T(8,128)(2,1)S(1)} %pad_maximum_fusion.near), channel_id=1, source_target_pairs={{0,24},{24,0},{8,16},{16,8},{1,25},{25,1},{9,17},{17,9},{2,26},{26... | collective-permute-start | bytes 1572872 | tf_op jit(solution)/shard_map/ppermute | solution.py:323
  68.6 1.9 %collective-permute-start.2 = (bf16[64,2048]{1,0:T(8,128)(2,1)S(1)}, bf16[64,2048]{1,0:T(8,128)(2,1)S(1)}, u32[]{:S(2)}, u32[]{:S(2)}) collective-permute-start(bf16[64,2048]{1,0:T(8,128)(2,1)S(1)} %bitcast.5), channel_id=1, source_target_pairs={{0,8},{8,0},{16,24},{24,16},{1,9},{9,1},{17,25},{25,17},{2,10},{10... | collective-permute-start | bytes 786440 | tf_op jit(solution)/shard_map/ppermute | solution.py:319
  70.6 0.6 reshape.11.gain_att
  71.1 6.6 %all-to-all-done.4.got = bf16[16,24,128]{2,1,0:T(8,128)(2,1)S(1)} async-done(((bf16[16,24,128]{2,1,0:T(8,128)(2,1)}), bf16[16,24,128]{2,1,0:T(8,128)(2,1)S(1)}, u32[]{:S(2)}, u32[]{:S(2)}) %all-to-all-start.4) | async-done | bytes 98336 | tf_op jit(solution)/shard_map/all_to_all | solution.py:22
  77.8 1.7 %shard_map.151 = f32[8,24,128]{2,1,0:T(8,128)} custom-call(bf16[16,24,128]{2,1,0:T(8,128)(2,1)S(1)} %all-to-all-done.4.got, bf16[4,144,128]{2,1,0:T(8,128)(2,1)S(1)} %all_to_all.46.w_all, bf16[1,256]{1,0:T(2,128)(2,1)} %reshape.11.gain_att), custom_call_target="tpu_custom_call" | custom-call | tf_op jit(solution)/shard_map/pallas_call | solution.py:298
  79.4 11.7 %all-to-all-start.5 = ((f32[8,24,128]{2,1,0:T(8,128)}), f32[8,24,128]{2,1,0:T(8,128)S(1)}, u32[]{:S(2)}, u32[]{:S(2)}) async-start(f32[8,24,128]{2,1,0:T(8,128)} %shard_map.151), calls=%async_computation.5 | async-start | bytes 196608 | tf_op jit(solution)/shard_map/all_to_all | solution.py:22
  91.2 4.9 %all-to-all-done.5.got = f32[8,24,128]{2,1,0:T(8,128)S(1)} async-done(((f32[8,24,128]{2,1,0:T(8,128)}), f32[8,24,128]{2,1,0:T(8,128)S(1)}, u32[]{:S(2)}, u32[]{:S(2)}) %all-to-all-start.5) | async-done | bytes 98336 | tf_op jit(solution)/shard_map/all_to_all | solution.py:22
  96.1 0.0 collective-permute-done.1.far
  96.1 0.4 shard_map.152
  96.5 2.8 %collective-permute-start.3 = (bf16[128,2048]{1,0:T(8,128)(2,1)S(1)}, bf16[128,2048]{1,0:T(8,128)(2,1)S(1)}, u32[]{:S(2)}, u32[]{:S(2)}) collective-permute-start(bf16[128,2048]{1,0:T(8,128)(2,1)S(1)} %pad_maximum_fusion.1.near), channel_id=1, source_target_pairs={{0,24},{24,0},{8,16},{16,8},{1,25},{25,1},{9,17},{17,9},{2,26},{26... | collective-permute-start | bytes 1572872 | tf_op jit(solution)/shard_map/ppermute | solution.py:323
  99.3 16.6 %all_to_all.47.got = bf16[16,16,128]{2,1,0:T(8,128)(2,1)S(1)} all-to-all(bf16[16,16,128]{2,1,0:T(8,128)(2,1)S(1)} %get-tuple-element.42), channel_id=1, replica_groups=mesh['z'=16,'y'=4,'tp'=8] {'z'}, dimensions={0} | all-to-all | bytes 131072 | tf_op jit(solution)/shard_map/all_to_all | solution.py:22
  115.9 0.2 shard_map.153
  116.1 14.3 %all_to_all.48.got = bf16[16,8,128]{2,1,0:T(8,128)(2,1)S(1)} all-to-all(bf16[16,8,128]{2,1,0:T(8,128)(2,1)S(1)} %shard_map.153), channel_id=1, replica_groups=mesh['z'=16,'y'=4,'tp'=8] {'z'}, dimensions={0} | all-to-all | bytes 65536 | tf_op jit(solution)/shard_map/all_to_all | solution.py:22
  130.4 0.0 collective-permute-done.3.far
  130.4 0.4 shard_map.154
  130.8 15.1 %all_to_all.49.got = f32[32,8,128]{2,1,0:T(8,128)S(1)} all-to-all(f32[32,8,128]{2,1,0:T(8,128)S(1)} %shard_map.154), channel_id=1, replica_groups=mesh['z'=16,'y'=4,'tp'=8] {'y','tp'}, dimensions={0} | all-to-all | bytes 262144 | tf_op jit(solution)/shard_map/all_to_all | solution.py:22
  145.9 0.6 copy.16
  (12 shorter events, 0.1 us)
Async XLA Ops:
  0.0 46.8 %copy-start = (s32[32]{0:T(128)S(1)}, s32[32]{0:T(128)}, u32[]{:S(2)}) copy-start(s32[32]{0:T(128)} %lengths.1) | copy-start | bytes 388
  12.2 26.9 %all-to-all-start.1 = ((bf16[16,32,128]{2,1,0:T(8,128)(2,1)}), bf16[16,32,128]{2,1,0:T(8,128)(2,1)S(1)}, u32[]{:S(2)}, u32[]{:S(2)}) async-start(bf16[16,32,128]{2,1,0:T(8,128)(2,1)} %get-tuple-element.26), calls=%async_computation.1 | async-start | bytes 262144 | tf_op jit(solution)/shard_map/all_to_all | solution.py:22
  27.2 12.3 %collective-permute-start = (bf16[64,2048]{1,0:T(8,128)(2,1)}, bf16[64,2048]{1,0:T(8,128)(2,1)S(1)}, u32[]{:S(2)}, u32[]{:S(2)}) collective-permute-start(bf16[64,2048]{1,0:T(8,128)(2,1)} %param.28), channel_id=1, source_target_pairs={{0,8},{8,0},{16,24},{24,16},{1,9},{9,1},{17,25},{25,17},{2,10},{10... | collective-permute-start | bytes 786440 | tf_op jit(solution)/shard_map/ppermute | solution.py:319
  46.8 7.3 %copy-start.1 = (bf16[64,2048]{1,0:T(8,128)(2,1)S(1)}, bf16[64,2048]{1,0:T(8,128)(2,1)}, u32[]{:S(2)}) copy-start(bf16[64,2048]{1,0:T(8,128)(2,1)} %param.28) | copy-start | bytes 786436
  46.8 21.9 %copy-start.2 = (bf16[2048,64]{0,1:T(8,128)(2,1)S(1)}, bf16[2048,64]{0,1:T(8,128)(2,1)}, u32[]{:S(2)}) copy-start(bf16[2048,64]{0,1:T(8,128)(2,1)} %param.29) | copy-start | bytes 786436
  46.8 23.8 %copy-start.3 = (bf16[256]{0:T(256)(128)(2,1)S(1)}, bf16[256]{0:T(256)(128)(2,1)}, u32[]{:S(2)}) copy-start(bf16[256]{0:T(256)(128)(2,1)} %param.25) | copy-start | bytes 1540
  50.8 7.7 %all-to-all-start.3 = ((f32[4,32,128]{2,1,0:T(8,128)}), f32[4,32,128]{2,1,0:T(8,128)S(1)}, u32[]{:S(2)}, u32[]{:S(2)}) async-start(f32[4,32,128]{2,1,0:T(8,128)} %shard_map.149), calls=%async_computation.3 | async-start | bytes 131072 | tf_op jit(solution)/shard_map/all_to_all | solution.py:22
  59.3 18.4 %all-to-all-start.4 = ((bf16[16,24,128]{2,1,0:T(8,128)(2,1)}), bf16[16,24,128]{2,1,0:T(8,128)(2,1)S(1)}, u32[]{:S(2)}, u32[]{:S(2)}) async-start(bf16[16,24,128]{2,1,0:T(8,128)(2,1)} %shard_map.150), calls=%async_computation.4 | async-start | bytes 196608 | tf_op jit(solution)/shard_map/all_to_all | solution.py:22
  65.8 30.3 %collective-permute-start.1 = (bf16[128,2048]{1,0:T(8,128)(2,1)S(1)}, bf16[128,2048]{1,0:T(8,128)(2,1)S(1)}, u32[]{:S(2)}, u32[]{:S(2)}) collective-permute-start(bf16[128,2048]{1,0:T(8,128)(2,1)S(1)} %pad_maximum_fusion.near), channel_id=1, source_target_pairs={{0,24},{24,0},{8,16},{16,8},{1,25},{25,1},{9,17},{17,9},{2,26},{26... | collective-permute-start | bytes 1572872 | tf_op jit(solution)/shard_map/ppermute | solution.py:323
  68.6 22.5 %collective-permute-start.2 = (bf16[64,2048]{1,0:T(8,128)(2,1)S(1)}, bf16[64,2048]{1,0:T(8,128)(2,1)S(1)}, u32[]{:S(2)}, u32[]{:S(2)}) collective-permute-start(bf16[64,2048]{1,0:T(8,128)(2,1)S(1)} %bitcast.5), channel_id=1, source_target_pairs={{0,8},{8,0},{16,24},{24,16},{1,9},{9,1},{17,25},{25,17},{2,10},{10... | collective-permute-start | bytes 786440 | tf_op jit(solution)/shard_map/ppermute | solution.py:319
  79.4 16.7 %all-to-all-start.5 = ((f32[8,24,128]{2,1,0:T(8,128)}), f32[8,24,128]{2,1,0:T(8,128)S(1)}, u32[]{:S(2)}, u32[]{:S(2)}) async-start(f32[8,24,128]{2,1,0:T(8,128)} %shard_map.151), calls=%async_computation.5 | async-start | bytes 196608 | tf_op jit(solution)/shard_map/all_to_all | solution.py:22
  96.5 33.9 %collective-permute-start.3 = (bf16[128,2048]{1,0:T(8,128)(2,1)S(1)}, bf16[128,2048]{1,0:T(8,128)(2,1)S(1)}, u32[]{:S(2)}, u32[]{:S(2)}) collective-permute-start(bf16[128,2048]{1,0:T(8,128)(2,1)S(1)} %pad_maximum_fusion.1.near), channel_id=1, source_target_pairs={{0,24},{24,0},{8,16},{16,8},{1,25},{25,1},{9,17},{17,9},{2,26},{26... | collective-permute-start | bytes 1572872 | tf_op jit(solution)/shard_map/ppermute | solution.py:323

commit v4 on v3

--- a/solution.py
+++ b/solution.py
@@ -85,16 +85,14 @@
     q = total[0:16].astype(BF16)
     x = jnp.where(lanes(8) < 3, total[48:56], 0.0)
     one = high(x)
-    two = high(x - one)
-    three = high(x - one - two)
-    extra = one + pltpu.roll(two, 4, 1) + pltpu.roll(three, 8, 1)
+    both = one + pltpu.roll(high(x - one), 3, 1)
+    both = jnp.transpose(jnp.concatenate([both, jnp.zeros((120, 128), F32)], axis=0))[0:8]
     row = lax.broadcasted_iota(jnp.int32, (8, 128), 0)
     for p in range(16):
         k = total[16 + p : 17 + p]
         v = total[32 + p : 33 + p]
-        own = jnp.where(row == 0, k, jnp.where(row == 1, v, 0.0))
         out[p, 0:16, :] = q
-        out[p, 16:32, :] = jnp.concatenate([extra, own], axis=0).astype(BF16)
+        out[p, 16:24, :] = jnp.where(row == 6, k, jnp.where(row == 7, v, both)).astype(BF16)
     left = lanes(8) < 64
     for k in range(2):
         stream_all[k] = jnp.where(left, got[2 * k, 56:64], got[2 * k + 1, 56:64])
@@ -106,8 +104,9 @@
     total = got[0].astype(F32)
     for k in range(1, 16):
         total = total + got[k].astype(F32)
-    x = total[16:24]
-    x = x + pltpu.roll(x, 124, 1) + pltpu.roll(x, 120, 1)
+    x = jnp.concatenate([total[16:24], jnp.zeros((120, 128), F32)], axis=0)
+    x = jnp.transpose(x)[0:8]
+    x = x + pltpu.roll(x, 125, 1)
     scale = lax.rsqrt(x[:, 0:1] / WIDTH + norm_eps)
     scale = jnp.concatenate([scale, scale], axis=0)
     gate = jnp.concatenate([x[:, 1:2], x[:, 2:3]], axis=0) * scale
@@ -115,8 +114,8 @@
     mine = row_is(16, z)
     scale_z = jnp.sum(jnp.where(mine, scale, 0.0), axis=0, keepdims=True)
     gate_z = jnp.sum(jnp.where(mine, gate, 0.0), axis=0, keepdims=True)
-    k = high(total[24:25] * scale_z)
-    v = high(total[25:26] * scale_z)
+    k = high(total[22:23] * scale_z)
+    v = high(total[23:24] * scale_z)
     q_z = jnp.sum(jnp.where(mine, q.astype(F32), 0.0), axis=0, keepdims=True)
     own = jnp.sum(q_z * k, axis=1, keepdims=True) * (1.0 / math.sqrt(128))
     own = own + jnp.maximum(-gate_z, 0.0) + jnp.log1p(jnp.exp(-jnp.abs(gate_z)))
@@ -218,7 +217,7 @@
             merged = merged + weight * got[k, 0:16, :].astype(F32)[h * 8 : h * 8 + 8]
         attended = merged / total
         squares = squares + jnp.sum(attended * attended, axis=1, keepdims=True)
-        attended_in = (attended * gain[:, h * 128 : h * 128 + 128]).astype(BF16)
+        attended_in = (attended * gain[h : h + 1]).astype(BF16)
         w = jnp.concatenate([w_all[y, 16 + h * 64 : 80 + h * 64, :] for y in range(4)], axis=0)
         part = part + dot_nt(attended_in, w)
     extra = columns([squares])
@@ -243,8 +242,8 @@
         halves[2 + k] = pltpu.roll(mixer_in, 64, 1)
         residual_out[2 * k] = residual
         residual_out[2 * k + 1] = pltpu.roll(residual, 64, 1)
-    up = dot(halves[y // 2 + 2 * (y % 2)].astype(BF16), near[...])
-    up = up + dot(halves[1 - y // 2 + 2 * (1 - y % 2)].astype(BF16), far[...])
+    up = dot(halves[y // 2 + 2 * (y % 2)].astype(BF16), near[0:128, :])
+    up = up + dot(halves[1 - y // 2 + 2 * (1 - y % 2)].astype(BF16), far[0:128, :])
     one = high(squares)
     two = high(squares - one)
     extra = columns([one, two, squares - one - two])
@@ -306,8 +305,8 @@
     return found if len(shapes) > 1 else found[0]
 
 
-def fetch(keys, w_out, decay, keys_out, w_out_out, decay_out, sems):
-    pairs = ((keys, keys_out), (w_out, w_out_out), (decay, decay_out))
+def fetch(keys, w_out, decay, gain, keys_out, w_out_out, decay_out, gain_out, sems):
+    pairs = ((keys, keys_out), (w_out, w_out_out), (decay, decay_out), (gain, gain_out))
     copies = [pltpu.make_async_copy(a, b, sems.at[k]) for k, (a, b) in enumerate(pairs)]
     for copy in copies:
         copy.start()
@@ -356,23 +355,25 @@
     )
     got = swap(lines, "y")
     lines, stream_all, gain_all = call(
-        spread_rows, [((16, 32, 128), BF16), ((2, 8, 128), F32), ((2, 8, 128), F32)], got
-    )
-    lines, w_up, keys_cache = lax.optimization_barrier((lines, w_up, keys_cache))
+        spread_rows, [((16, 24, 128), BF16), ((2, 8, 128), F32), ((2, 8, 128), F32)], got
+    )
+    lines, keys_cache = lax.optimization_barrier((lines, keys_cache))
     got = swap(lines, "z")
-    keys, w_out, decay = call(
+    keys, w_out, decay, gain_att = call(
         fetch,
-        [(keys_cache.shape, BF16), ((64, 256), BF16), (decay_cache.shape, F32)],
+        [(keys_cache.shape, BF16), ((64, 256), BF16), (decay_cache.shape, F32), ((2, 128), BF16)],
         keys_cache,
         w_out.T,
         decay_cache,
+        gain_att.reshape(2, 128),
         near=(),
-        anywhere=(0, 1, 2),
-        scratch=(pltpu.SemaphoreType.DMA((3,)),),
+        anywhere=(0, 1, 2, 3),
+        scratch=(pltpu.SemaphoreType.DMA((4,)),),
     )
     other = beside(w_up)
     lines, own = call(finish_rows, [((4, 144, 128), BF16), ((8, 128), F32)], got, w_out, near=(0, 1))
     lines, other = lax.optimization_barrier((lines, other))
+    up_near = jnp.concatenate([w_up, other], axis=0)
     w_all = swap(lines, "y")
     lines = call(
         attend,
@@ -387,14 +388,14 @@
         scalars=(4,),
         scratch=(pltpu.VMEM((32, 2, 128, 128), BF16), pltpu.SemaphoreType.DMA((4,))),
     )
+    lines, up_near = lax.optimization_barrier((lines, up_near))
     got = swap(lines, "y")
+    up_far = across(up_near)
     lines = call(merge_blocks, [((16, 24, 128), BF16)], got, own, near=(0, 1))
-    up_near = jnp.concatenate([w_up, other], axis=0)
-    lines, up_near, w_down = lax.optimization_barrier((lines, up_near, w_down.T))
+    lines, w_down = lax.optimization_barrier((lines, w_down.T))
     got = swap(lines, "z")
-    up_far = across(up_near)
     other = beside(w_down)
-    lines = call(project_out, [((8, 24, 128), F32)], got, w_all, gain_att.reshape(1, 256), near=(0, 1))
+    lines = call(project_out, [((8, 24, 128), F32)], got, w_all, gain_att, near=(0, 1, 2))
     got = swap(lines, "tp")
     lines, residual = call(
         mix_up,

time: 147 us -> 146 us (level)
  no operation moved by 1% of the time
where the time goes in v4:
time: 146 us; the launch traced here: 145 us
  blocking collectives  61.9 us (42%)
  starting transfers between devices  45.8 us (31%)
  waiting for transfers between devices  25 us (17%)
  Pallas kernels  11.4 us (8%)
    all_to_all x5, blocking collectives, swap(): return lax.all_to_all(value, axis, split_axis=0, concat_axis=0, tiled=True)  61.9 us
    all_to_all x4, starting transfers between devices, swap(): return lax.all_to_all(value, axis, split_axis=0, concat_axis=0, tiled=True)  36 us
    all_to_all x4, waiting for transfers between devices, swap(): return lax.all_to_all(value, axis, split_axis=0, concat_axis=0, tiled=True)  24.9 us
    pallas_call x11, Pallas kernels, call(): pl.pallas_call(kernel, out_shape=shapes, in_specs=specs, out_specs=[pl.Bl...  11.4 us
    ppermute x2, starting transfers between devices, across(): return lax.ppermute(value, 'y', [(0, 3), (3, 0), (1, 2), (2, 1)])  5.59 us
    ppermute x2, starting transfers between devices, beside(): return lax.ppermute(value, 'y', [(0, 1), (1, 0), (2, 3), (3, 2)])  4.12 us
  transfers between devices with their start and end apart: 8, of which 4 were waited for; matrix products, arithmetic and copies ran while one was open for 0% of the time, Pallas kernels for 3%

profile of v4, /device:TPU:1, one launch (start us, length us, event | category | flops | bytes accessed | tf_op | source)
XLA Modules:
  0.0 144.8 jit_solution(1378893602554257904)
XLA Ops:
  0.0 1.9 %shard_map.145 = f32[4,64,128]{2,1,0:T(8,128)S(1)} custom-call(bf16[32,64]{1,0:T(8,128)(2,1)} %stream.1, bf16[1,64]{1,0:T(2,128)(2,1)} %bitcast.10, bf16[1,64]{1,0:T(2,128)(2,1)} %bitcast.11, bf16[64,256]{1,0:T(8,128)(2,1)} %w_query.1, bf16[64,256]{1,0:T(8,128)(2,1)} %w_key.1, bf16[64,256]{1,0:T(8,128)(2,1)} %w_value.1, bf16[16,4096]{1,0:T(8,128)(2,1)} %bitcast.8), custom_call_target="tpu_custom_call" | custom-call | tf_op jit(solution)/shard_map/pallas_call | solution.py:297
  1.9 0.0 copy-start
  1.9 9.6 %all_to_all.45.got = f32[4,64,128]{2,1,0:T(8,128)S(1)} all-to-all(f32[4,64,128]{2,1,0:T(8,128)S(1)} %shard_map.145), channel_id=1, replica_groups=mesh['z'=16,'y'=4,'tp'=8] {'y'}, dimensions={0} | all-to-all | bytes 262144 | tf_op jit(solution)/shard_map/all_to_all | solution.py:22
  11.5 0.8 shard_map.146
  12.3 14.9 %all-to-all-start.1 = ((bf16[16,24,128]{2,1,0:T(8,128)(2,1)}), bf16[16,24,128]{2,1,0:T(8,128)(2,1)S(1)}, u32[]{:S(2)}, u32[]{:S(2)}) async-start(bf16[16,24,128]{2,1,0:T(8,128)(2,1)} %get-tuple-element.27), calls=%async_computation.1 | async-start | bytes 196608 | tf_op jit(solution)/shard_map/all_to_all | solution.py:22
  27.3 2.2 %collective-permute-start = (bf16[64,2048]{1,0:T(8,128)(2,1)}, bf16[64,2048]{1,0:T(8,128)(2,1)S(1)}, u32[]{:S(2)}, u32[]{:S(2)}) collective-permute-start(bf16[64,2048]{1,0:T(8,128)(2,1)} %param.28), channel_id=1, source_target_pairs={{0,8},{8,0},{16,24},{24,16},{1,9},{9,1},{17,25},{25,17},{2,10},{10... | collective-permute-start | bytes 786440 | tf_op jit(solution)/shard_map/ppermute | solution.py:318
  29.5 1.6 %shard_map.147 = (bf16[32,2,128,128]{3,2,1,0:T(8,128)(2,1)S(1)}, bf16[64,256]{1,0:T(8,128)(2,1)S(1)}, f32[32,2,128]{2,1,0:T(2,128)S(1)}, bf16[2,128]{1,0:T(2,128)(2,1)S(1)}) custom-call(bf16[32,2,128,128]{3,2,1,0:T(8,128)(2,1)} %keys, bf16[64,256]{1,0:T(8,128)(2,1)} %bitcast.9, f32[32,2,128]{2,1,0:T(2,128)} %decay.1, bf16[2,128]{1,0:T(2,128)(2,1)} %bitcast.12), custom_call_target="tpu_custom_call" | custom-call | tf_op jit(solution)/shard_map/pallas_call | solution.py:297
  31.1 8.0 %all-to-all-done.1.got = bf16[16,24,128]{2,1,0:T(8,128)(2,1)S(1)} async-done(((bf16[16,24,128]{2,1,0:T(8,128)(2,1)}), bf16[16,24,128]{2,1,0:T(8,128)(2,1)S(1)}, u32[]{:S(2)}, u32[]{:S(2)}) %all-to-all-start.1) | async-done | bytes 98336 | tf_op jit(solution)/shard_map/all_to_all | solution.py:22
  39.1 0.9 shard_map.148
  40.0 0.0 collective-permute-done
  40.0 3.3 %all-to-all-start.2 = ((bf16[4,144,128]{2,1,0:T(8,128)(2,1)}), bf16[4,144,128]{2,1,0:T(8,128)(2,1)S(1)}, u32[]{:S(2)}, u32[]{:S(2)}) async-start(bf16[4,144,128]{2,1,0:T(8,128)(2,1)} %get-tuple-element.31), calls=%async_computation.2 | async-start | bytes 294912 | tf_op jit(solution)/shard_map/all_to_all | solution.py:22
  43.4 4.8 %all-to-all-done.2.w_all = bf16[4,144,128]{2,1,0:T(8,128)(2,1)S(1)} async-done(((bf16[4,144,128]{2,1,0:T(8,128)(2,1)}), bf16[4,144,128]{2,1,0:T(8,128)(2,1)S(1)}, u32[]{:S(2)}, u32[]{:S(2)}) %all-to-all-start.2) | async-done | bytes 147488 | tf_op jit(solution)/shard_map/all_to_all | solution.py:22
  48.2 3.4 %shard_map.149 = f32[4,32,128]{2,1,0:T(8,128)S(1)} custom-call(bf16[4,144,128]{2,1,0:T(8,128)(2,1)S(1)} %all-to-all-done.2.w_all, bf16[32,2,128,128]{3,2,1,0:T(8,128)(2,1)S(1)} %get-tuple-element.32.keys, bf16[32,2,128,128]{3,2,1,0:T(8,128)(2,1)} %values_far.1, f32[32,2,128]{2,1,0:T(2,128)S(1)} %get-tuple-element.33.decay, s32[32]{0:T(128)S(1)} %copy-done), custom_call_target="tpu_custom_call" | custom-call | tf_op jit(solution)/shard_map/pallas_call | solution.py:297
  51.6 6.8 %all_to_all.46.got = f32[4,32,128]{2,1,0:T(8,128)S(1)} all-to-all(f32[4,32,128]{2,1,0:T(8,128)S(1)} %shard_map.149), channel_id=1, replica_groups=mesh['z'=16,'y'=4,'tp'=8] {'y'}, dimensions={0} | all-to-all | bytes 131072 | tf_op jit(solution)/shard_map/all_to_all | solution.py:22
  58.5 0.8 shard_map.150
  59.3 6.0 %all-to-all-start.4 = ((bf16[16,24,128]{2,1,0:T(8,128)(2,1)}), bf16[16,24,128]{2,1,0:T(8,128)(2,1)S(1)}, u32[]{:S(2)}, u32[]{:S(2)}) async-start(bf16[16,24,128]{2,1,0:T(8,128)(2,1)} %shard_map.150), calls=%async_computation.4 | async-start | bytes 196608 | tf_op jit(solution)/shard_map/all_to_all | solution.py:22
  65.3 2.8 %collective-permute-start.1 = (bf16[128,2048]{1,0:T(8,128)(2,1)S(1)}, bf16[128,2048]{1,0:T(8,128)(2,1)S(1)}, u32[]{:S(2)}, u32[]{:S(2)}) collective-permute-start(bf16[128,2048]{1,0:T(8,128)(2,1)S(1)} %pad_maximum_fusion.near), channel_id=1, source_target_pairs={{0,24},{24,0},{8,16},{16,8},{1,25},{25,1},{9,17},{17,9},{2,26},{26... | collective-permute-start | bytes 1572872 | tf_op jit(solution)/shard_map/ppermute | solution.py:322
  68.1 1.9 %collective-permute-start.2 = (bf16[64,2048]{1,0:T(8,128)(2,1)S(1)}, bf16[64,2048]{1,0:T(8,128)(2,1)S(1)}, u32[]{:S(2)}, u32[]{:S(2)}) collective-permute-start(bf16[64,2048]{1,0:T(8,128)(2,1)S(1)} %bitcast.6), channel_id=1, source_target_pairs={{0,8},{8,0},{16,24},{24,16},{1,9},{9,1},{17,25},{25,17},{2,10},{10... | collective-permute-start | bytes 786440 | tf_op jit(solution)/shard_map/ppermute | solution.py:318
  70.0 7.2 %all-to-all-done.4.got = bf16[16,24,128]{2,1,0:T(8,128)(2,1)S(1)} async-done(((bf16[16,24,128]{2,1,0:T(8,128)(2,1)}), bf16[16,24,128]{2,1,0:T(8,128)(2,1)S(1)}, u32[]{:S(2)}, u32[]{:S(2)}) %all-to-all-start.4) | async-done | bytes 98336 | tf_op jit(solution)/shard_map/all_to_all | solution.py:22
  77.2 1.0 shard_map.151
  78.2 11.8 %all-to-all-start.5 = ((f32[8,24,128]{2,1,0:T(8,128)}), f32[8,24,128]{2,1,0:T(8,128)S(1)}, u32[]{:S(2)}, u32[]{:S(2)}) async-start(f32[8,24,128]{2,1,0:T(8,128)} %shard_map.151), calls=%async_computation.5 | async-start | bytes 196608 | tf_op jit(solution)/shard_map/all_to_all | solution.py:22
  90.0 0.0 collective-permute-done.2
  90.1 4.9 %all-to-all-done.5.got = f32[8,24,128]{2,1,0:T(8,128)S(1)} async-done(((f32[8,24,128]{2,1,0:T(8,128)}), f32[8,24,128]{2,1,0:T(8,128)S(1)}, u32[]{:S(2)}, u32[]{:S(2)}) %all-to-all-start.5) | async-done | bytes 98336 | tf_op jit(solution)/shard_map/all_to_all | solution.py:22
  95.0 0.0 collective-permute-done.1.far
  95.0 0.4 shard_map.152
  95.4 2.8 %collective-permute-start.3 = (bf16[128,2048]{1,0:T(8,128)(2,1)S(1)}, bf16[128,2048]{1,0:T(8,128)(2,1)S(1)}, u32[]{:S(2)}, u32[]{:S(2)}) collective-permute-start(bf16[128,2048]{1,0:T(8,128)(2,1)S(1)} %pad_maximum_fusion.1.near), channel_id=1, source_target_pairs={{0,24},{24,0},{8,16},{16,8},{1,25},{25,1},{9,17},{17,9},{2,26},{26... | collective-permute-start | bytes 1572872 | tf_op jit(solution)/shard_map/ppermute | solution.py:322
  98.2 16.0 %all_to_all.47.got = bf16[16,16,128]{2,1,0:T(8,128)(2,1)S(1)} all-to-all(bf16[16,16,128]{2,1,0:T(8,128)(2,1)S(1)} %get-tuple-element.44), channel_id=1, replica_groups=mesh['z'=16,'y'=4,'tp'=8] {'z'}, dimensions={0} | all-to-all | bytes 131072 | tf_op jit(solution)/shard_map/all_to_all | solution.py:22
  114.2 0.2 shard_map.153
  114.4 14.3 %all_to_all.48.got = bf16[16,8,128]{2,1,0:T(8,128)(2,1)S(1)} all-to-all(bf16[16,8,128]{2,1,0:T(8,128)(2,1)S(1)} %shard_map.153), channel_id=1, replica_groups=mesh['z'=16,'y'=4,'tp'=8] {'z'}, dimensions={0} | all-to-all | bytes 65536 | tf_op jit(solution)/shard_map/all_to_all | solution.py:22
  128.7 0.4 shard_map.154
  129.1 15.1 %all_to_all.49.got = f32[32,8,128]{2,1,0:T(8,128)S(1)} all-to-all(f32[32,8,128]{2,1,0:T(8,128)S(1)} %shard_map.154), channel_id=1, replica_groups=mesh['z'=16,'y'=4,'tp'=8] {'y','tp'}, dimensions={0} | all-to-all | bytes 262144 | tf_op jit(solution)/shard_map/all_to_all | solution.py:22
  144.2 0.6 copy.16
  (9 shorter events, 0.1 us)
Async XLA Ops:
  0.0 43.4 %copy-start.1 = (bf16[64,2048]{1,0:T(8,128)(2,1)S(1)}, bf16[64,2048]{1,0:T(8,128)(2,1)}, u32[]{:S(2)}) copy-start(bf16[64,2048]{1,0:T(8,128)(2,1)} %param.28) | copy-start | bytes 786436
  1.9 46.3 %copy-start = (s32[32]{0:T(128)S(1)}, s32[32]{0:T(128)}, u32[]{:S(2)}) copy-start(s32[32]{0:T(128)} %lengths.1) | copy-start | bytes 388
  12.3 26.8 %all-to-all-start.1 = ((bf16[16,24,128]{2,1,0:T(8,128)(2,1)}), bf16[16,24,128]{2,1,0:T(8,128)(2,1)S(1)}, u32[]{:S(2)}, u32[]{:S(2)}) async-start(bf16[16,24,128]{2,1,0:T(8,128)(2,1)} %get-tuple-element.27), calls=%async_computation.1 | async-start | bytes 196608 | tf_op jit(solution)/shard_map/all_to_all | solution.py:22
  27.3 12.8 %collective-permute-start = (bf16[64,2048]{1,0:T(8,128)(2,1)}, bf16[64,2048]{1,0:T(8,128)(2,1)S(1)}, u32[]{:S(2)}, u32[]{:S(2)}) collective-permute-start(bf16[64,2048]{1,0:T(8,128)(2,1)} %param.28), channel_id=1, source_target_pairs={{0,8},{8,0},{16,24},{24,16},{1,9},{9,1},{17,25},{25,17},{2,10},{10... | collective-permute-start | bytes 786440 | tf_op jit(solution)/shard_map/ppermute | solution.py:318
  40.0 8.2 %all-to-all-start.2 = ((bf16[4,144,128]{2,1,0:T(8,128)(2,1)}), bf16[4,144,128]{2,1,0:T(8,128)(2,1)S(1)}, u32[]{:S(2)}, u32[]{:S(2)}) async-start(bf16[4,144,128]{2,1,0:T(8,128)(2,1)} %get-tuple-element.31), calls=%async_computation.2 | async-start | bytes 294912 | tf_op jit(solution)/shard_map/all_to_all | solution.py:22
  48.2 19.9 %copy-start.2 = (bf16[2048,64]{0,1:T(8,128)(2,1)S(1)}, bf16[2048,64]{0,1:T(8,128)(2,1)}, u32[]{:S(2)}) copy-start(bf16[2048,64]{0,1:T(8,128)(2,1)} %param.29) | copy-start | bytes 786436
  59.3 18.0 %all-to-all-start.4 = ((bf16[16,24,128]{2,1,0:T(8,128)(2,1)}), bf16[16,24,128]{2,1,0:T(8,128)(2,1)S(1)}, u32[]{:S(2)}, u32[]{:S(2)}) async-start(bf16[16,24,128]{2,1,0:T(8,128)(2,1)} %shard_map.150), calls=%async_computation.4 | async-start | bytes 196608 | tf_op jit(solution)/shard_map/all_to_all | solution.py:22
  65.3 29.7 %collective-permute-start.1 = (bf16[128,2048]{1,0:T(8,128)(2,1)S(1)}, bf16[128,2048]{1,0:T(8,128)(2,1)S(1)}, u32[]{:S(2)}, u32[]{:S(2)}) collective-permute-start(bf16[128,2048]{1,0:T(8,128)(2,1)S(1)} %pad_maximum_fusion.near), channel_id=1, source_target_pairs={{0,24},{24,0},{8,16},{16,8},{1,25},{25,1},{9,17},{17,9},{2,26},{26... | collective-permute-start | bytes 1572872 | tf_op jit(solution)/shard_map/ppermute | solution.py:322
  68.1 21.9 %collective-permute-start.2 = (bf16[64,2048]{1,0:T(8,128)(2,1)S(1)}, bf16[64,2048]{1,0:T(8,128)(2,1)S(1)}, u32[]{:S(2)}, u32[]{:S(2)}) collective-permute-start(bf16[64,2048]{1,0:T(8,128)(2,1)S(1)} %bitcast.6), channel_id=1, source_target_pairs={{0,8},{8,0},{16,24},{24,16},{1,9},{9,1},{17,25},{25,17},{2,10},{10... | collective-permute-start | bytes 786440 | tf_op jit(solution)/shard_map/ppermute | solution.py:318
  78.2 16.8 %all-to-all-start.5 = ((f32[8,24,128]{2,1,0:T(8,128)}), f32[8,24,128]{2,1,0:T(8,128)S(1)}, u32[]{:S(2)}, u32[]{:S(2)}) async-start(f32[8,24,128]{2,1,0:T(8,128)} %shard_map.151), calls=%async_computation.5 | async-start | bytes 196608 | tf_op jit(solution)/shard_map/all_to_all | solution.py:22
  95.4 33.3 %collective-permute-start.3 = (bf16[128,2048]{1,0:T(8,128)(2,1)S(1)}, bf16[128,2048]{1,0:T(8,128)(2,1)S(1)}, u32[]{:S(2)}, u32[]{:S(2)}) collective-permute-start(bf16[128,2048]{1,0:T(8,128)(2,1)S(1)} %pad_maximum_fusion.1.near), channel_id=1, source_target_pairs={{0,24},{24,0},{8,16},{16,8},{1,25},{25,1},{9,17},{17,9},{2,26},{26... | collective-permute-start | bytes 1572872 | tf_op jit(solution)/shard_map/ppermute | solution.py:322

commit v5 on v4

--- a/solution.py
+++ b/solution.py
@@ -140,10 +140,7 @@
     for y in range(4):
         q = w_all[y, 0:16, :]
         every = dot_nt(q, keys[y * 8 : y * 8 + 8].reshape(2048, 128))
-        length = jnp.zeros((8, 128), jnp.int32)
-        for b in range(8):
-            length = jnp.where(row == b, lengths[y * 8 + b], length)
-        live = place < length
+        live = place < lengths[y]
         probs = []
         for h in range(2):
             s = jnp.zeros((8, 128), F32)
@@ -163,7 +160,8 @@
                 none = jnp.zeros((8, 128), F32)
                 wide.append(jnp.concatenate([own, none] if h == 0 else [none, own], axis=0).astype(BF16))
         copies[y].wait()
-        out[y, 0:16, :] = dot(jnp.concatenate(wide, axis=1), values[y * 8 : y * 8 + 8].reshape(2048, 128))
+        found = values[y * 8 : y * 8 + 8].reshape(2048, 128)
+        out[y, 0:16, :] = dot(jnp.concatenate(wide, axis=1), found)
 
 
 def merge_blocks(got, own, out):
@@ -227,7 +225,9 @@
         out[k, 16:24, :] = extra
 
 
-def mix_up(got, stream_all, gain_all, near, far, out, residual_out, halves):
+def mix_up(got, stream_all, gain_all, near, far, w_down, other, out, residual_out, down_near, halves):
+    down_near[0:64, :] = w_down[...]
+    down_near[64:128, :] = other[...]
     y = lax.axis_index("y")
     total = got[0]
     for k in range(1, 8):
@@ -284,7 +284,7 @@
         out[y * 8 : y * 8 + 8, :] = total[:, 0:64].astype(BF16)
 
 
-def call(kernel, outs, *args, near=(0,), anywhere=(), scalars=(), scratch=()):
+def call(kernel, outs, *args, near=(0,), anywhere=(), scalars=(), scratch=(), place=pltpu.VMEM):
     specs = []
     placed = []
     for k, a in enumerate(args):
@@ -293,7 +293,7 @@
         if k not in scalars:
             a = pltpu.with_memory_space_constraint(a, pltpu.VMEM if k in near else pltpu.HBM)
         placed.append(a)
-    shapes = [pltpu.VMEM(s, d) for s, d in outs]
+    shapes = [place(s, d) for s, d in outs]
     found = pl.pallas_call(
         kernel,
         out_shape=shapes,
@@ -305,11 +305,27 @@
     return found if len(shapes) > 1 else found[0]
 
 
-def fetch(keys, w_out, decay, gain, keys_out, w_out_out, decay_out, gain_out, sems):
-    pairs = ((keys, keys_out), (w_out, w_out_out), (decay, decay_out), (gain, gain_out))
+def fetch(
+    keys, w_out, decay, gain, w_up, other, lengths,
+    keys_out, w_out_out, decay_out, gain_out, near, lengths_out, sems,
+):
+    pairs = (
+        (keys, keys_out),
+        (w_out, w_out_out),
+        (decay, decay_out),
+        (gain, gain_out),
+        (w_up, near.at[0:64]),
+    )
     copies = [pltpu.make_async_copy(a, b, sems.at[k]) for k, (a, b) in enumerate(pairs)]
     for copy in copies:
         copy.start()
+    near[64:128, :] = other[...]
+    row = lax.broadcasted_iota(jnp.int32, (8, 128), 0)
+    for y in range(4):
+        length = jnp.zeros((8, 128), jnp.int32)
+        for b in range(8):
+            length = jnp.where(row == b, lengths[y * 8 + b], length)
+        lengths_out[y] = length
     for copy in copies:
         copy.wait()
 
@@ -359,21 +375,30 @@
     )
     lines, keys_cache = lax.optimization_barrier((lines, keys_cache))
     got = swap(lines, "z")
-    keys, w_out, decay, gain_att = call(
+    other = beside(w_up)
+    keys, w_out, decay, gain_att, up_near, lengths = call(
         fetch,
-        [(keys_cache.shape, BF16), ((64, 256), BF16), (decay_cache.shape, F32), ((2, 128), BF16)],
+        [
+            (keys_cache.shape, BF16),
+            ((64, 256), BF16),
+            (decay_cache.shape, F32),
+            ((2, 128), BF16),
+            ((128, 2048), BF16),
+            ((4, 8, 128), jnp.int32),
+        ],
         keys_cache,
         w_out.T,
         decay_cache,
         gain_att.reshape(2, 128),
-        near=(),
-        anywhere=(0, 1, 2, 3),
-        scratch=(pltpu.SemaphoreType.DMA((4,)),),
-    )
-    other = beside(w_up)
+        w_up,
+        other,
+        lengths,
+        near=(5,),
+        anywhere=(0, 1, 2, 3, 4),
+        scalars=(6,),
+        scratch=(pltpu.SemaphoreType.DMA((5,)),),
+    )
     lines, own = call(finish_rows, [((4, 144, 128), BF16), ((8, 128), F32)], got, w_out, near=(0, 1))
-    lines, other = lax.optimization_barrier((lines, other))
-    up_near = jnp.concatenate([w_up, other], axis=0)
     w_all = swap(lines, "y")
     lines = call(
         attend,
@@ -383,9 +408,8 @@
         values_cache,
         decay,
         lengths,
-        near=(0, 1, 3),
+        near=(0, 1, 3, 4),
         anywhere=(2,),
-        scalars=(4,),
         scratch=(pltpu.VMEM((32, 2, 128, 128), BF16), pltpu.SemaphoreType.DMA((4,))),
     )
     lines, up_near = lax.optimization_barrier((lines, up_near))
@@ -397,25 +421,25 @@
     other = beside(w_down)
     lines = call(project_out, [((8, 24, 128), F32)], got, w_all, gain_att, near=(0, 1, 2))
     got = swap(lines, "tp")
-    lines, residual = call(
+    lines, residual, down_near = call(
         mix_up,
-        [((16, 16, 128), BF16), ((4, 8, 128), F32)],
+        [((16, 16, 128), BF16), ((4, 8, 128), F32), ((128, 2048), BF16)],
         got,
         stream_all,
         gain_all,
         up_near,
         up_far,
-        near=tuple(range(5)),
+        w_down,
+        other,
+        near=tuple(range(7)),
         scratch=(pltpu.VMEM((4, 8, 128), F32),),
     )
-    down_near = jnp.concatenate([w_down, other], axis=0)
-    lines, down_near = lax.optimization_barrier((lines, down_near))
     got = swap(lines, "z")
     down_far = across(down_near)
     got = swap(call(activate, [((16, 8, 128), BF16)], got), "z")
     lines = call(mix_down, [((32, 8, 128), F32)], got, residual, down_near, down_far, near=tuple(range(4)))
     got = swap(lines, ("y", "tp"))
-    return call(finish, [((32, 64), BF16)], got)
+    return call(finish, [((32, 64), BF16)], got, place=pltpu.HBM)
 
 
 def solution(mesh):

time: 146 us -> 151 us (1.034)
  blocking collectives: 61.9 us -> 70.5 us
  waiting for transfers between devices: 25 us -> 21.7 us
    all_to_all x4 -> x3, waiting for transfers between devices: 24.9 us -> 16.2 us  [swap(): return lax.all_to_all(value, axis, split_axis=0, concat_axis=0, tiled=True)]
    all_to_all x5 -> x6, blocking collectives: 61.9 us -> 70.5 us  [swap(): return lax.all_to_all(value, axis, split_axis=0, concat_axis=0, tiled=True)]
    ppermute x2, waiting for transfers between devices: 0.01 us -> 5.42 us  [beside(): return lax.ppermute(value, 'y', [(0, 1), (1, 0), (2, 3), (3, 2)])]
    all_to_all x4 -> x3, starting transfers between devices: 36 us -> 36.2 us  [swap(): return lax.all_to_all(value, axis, split_axis=0, concat_axis=0, tiled=True)]
  transfers between devices with their start and end apart: 8 -> 7, of which waited for: 4 -> 4; matrix products, arithmetic and copies ran while one was open for 0% -> 0% of each run, Pallas kernels for 3% -> 3%
where the time goes in v5:
time: 151 us; the launch traced here: 150 us
  blocking collectives  70.5 us (47%)
  starting transfers between devices  45.9 us (30%)
  waiting for transfers between devices  21.7 us (14%)
  Pallas kernels  11.4 us (8%)
    all_to_all x6, blocking collectives, swap(): return lax.all_to_all(value, axis, split_axis=0, concat_axis=0, tiled=True)  70.5 us
    all_to_all x3, starting transfers between devices, swap(): return lax.all_to_all(value, axis, split_axis=0, concat_axis=0, tiled=True)  36.2 us
    all_to_all x3, waiting for transfers between devices, swap(): return lax.all_to_all(value, axis, split_axis=0, concat_axis=0, tiled=True)  16.2 us
    pallas_call x11, Pallas kernels, call(): pl.pallas_call(kernel, out_shape=shapes, in_specs=specs, out_specs=[pl.Bl...  11.4 us
    ppermute x2, starting transfers between devices, across(): return lax.ppermute(value, 'y', [(0, 3), (3, 0), (1, 2), (2, 1)])  5.59 us
    ppermute x2, waiting for transfers between devices, beside(): return lax.ppermute(value, 'y', [(0, 1), (1, 0), (2, 3), (3, 2)])  5.42 us
    ppermute x2, starting transfers between devices, beside(): return lax.ppermute(value, 'y', [(0, 1), (1, 0), (2, 3), (3, 2)])  4.12 us
  transfers between devices with their start and end apart: 7, of which 4 were waited for; matrix products, arithmetic and copies ran while one was open for 0% of the time, Pallas kernels for 3%

profile of v5, /device:TPU:1, one launch (start us, length us, event | category | flops | bytes accessed | tf_op | source)
XLA Modules:
  0.0 150.3 jit_solution(8281014594859954169)
XLA Ops:
  0.0 1.8 %shard_map.145 = f32[4,64,128]{2,1,0:T(8,128)S(1)} custom-call(bf16[32,64]{1,0:T(8,128)(2,1)} %stream.1, bf16[1,64]{1,0:T(2,128)(2,1)} %bitcast.10, bf16[1,64]{1,0:T(2,128)(2,1)} %bitcast.11, bf16[64,256]{1,0:T(8,128)(2,1)} %w_query.1, bf16[64,256]{1,0:T(8,128)(2,1)} %w_key.1, bf16[64,256]{1,0:T(8,128)(2,1)} %w_value.1, bf16[16,4096]{1,0:T(8,128)(2,1)} %bitcast.8), custom_call_target="tpu_custom_call" | custom-call | tf_op jit(solution)/shard_map/pallas_call | solution.py:297
  1.8 9.6 %all_to_all.45.got = f32[4,64,128]{2,1,0:T(8,128)S(1)} all-to-all(f32[4,64,128]{2,1,0:T(8,128)S(1)} %shard_map.145), channel_id=1, replica_groups=mesh['z'=16,'y'=4,'tp'=8] {'y'}, dimensions={0} | all-to-all | bytes 262144 | tf_op jit(solution)/shard_map/all_to_all | solution.py:22
  11.5 0.8 shard_map.146
  12.3 14.9 %all-to-all-start.1 = ((bf16[16,24,128]{2,1,0:T(8,128)(2,1)}), bf16[16,24,128]{2,1,0:T(8,128)(2,1)S(1)}, u32[]{:S(2)}, u32[]{:S(2)}) async-start(bf16[16,24,128]{2,1,0:T(8,128)(2,1)} %get-tuple-element.26), calls=%async_computation.1 | async-start | bytes 196608 | tf_op jit(solution)/shard_map/all_to_all | solution.py:22
  27.2 2.2 %collective-permute-start = (bf16[64,2048]{1,0:T(8,128)(2,1)}, bf16[64,2048]{1,0:T(8,128)(2,1)S(1)}, u32[]{:S(2)}, u32[]{:S(2)}) collective-permute-start(bf16[64,2048]{1,0:T(8,128)(2,1)} %w_up.1), channel_id=1, source_target_pairs={{0,8},{8,0},{16,24},{24,16},{1,9},{9,1},{17,25},{25,17},{2,10},{10... | collective-permute-start | bytes 786440 | tf_op jit(solution)/shard_map/ppermute | solution.py:334
  29.4 5.4 %collective-permute-done.other = bf16[64,2048]{1,0:T(8,128)(2,1)S(1)} collective-permute-done((bf16[64,2048]{1,0:T(8,128)(2,1)}, bf16[64,2048]{1,0:T(8,128)(2,1)S(1)}, u32[]{:S(2)}, u32[]{:S(2)}) %collective-permute-start) | collective-permute-done | bytes 262176 | tf_op jit(solution)/shard_map/ppermute | solution.py:334
  34.8 0.7 copy-done.1
  35.5 2.2 %shard_map.147 = (bf16[32,2,128,128]{3,2,1,0:T(8,128)(2,1)S(1)}, bf16[64,256]{1,0:T(8,128)(2,1)S(1)}, f32[32,2,128]{2,1,0:T(2,128)S(1)}, bf16[2,128]{1,0:T(2,128...) custom-call(bf16[32,2,128,128]{3,2,1,0:T(8,128)(2,1)} %keys, bf16[64,256]{1,0:T(8,128)(2,1)} %bitcast.9, ...), custom_call_target="tpu_custom_call" | custom-call | tf_op jit(solution)/shard_map/pallas_call | solution.py:297
  37.7 1.3 all-to-all-done.1.got
  39.0 0.4 shard_map.148
  39.5 7.3 %all_to_all.46.w_all = bf16[4,144,128]{2,1,0:T(8,128)(2,1)S(1)} all-to-all(bf16[4,144,128]{2,1,0:T(8,128)(2,1)S(1)} %get-tuple-element.29), channel_id=1, replica_groups=mesh['z'=16,'y'=4,'tp'=8] {'y'}, dimensions={0} | all-to-all | bytes 294912 | tf_op jit(solution)/shard_map/all_to_all | solution.py:22
  46.7 2.8 %shard_map.149 = f32[4,32,128]{2,1,0:T(8,128)S(1)} custom-call(bf16[4,144,128]{2,1,0:T(8,128)(2,1)S(1)} %all_to_all.46.w_all, bf16[32,2,128,128]{3,2,1,0:T(8,128)(2,1)S(1)} %get-tuple-element.30.keys, bf16[32,2,128,128]{3,2,1,0:T(8,128)(2,1)} %values_far.1, f32[32,2,128]{2,1,0:T(2,128)S(1)} %get-tuple-element.31.decay, ...), custom_call_target="tpu_custom_call" | custom-call | tf_op jit(solution)/shard_map/pallas_call | solution.py:297
  49.5 2.8 %collective-permute-start.1 = (bf16[128,2048]{1,0:T(8,128)(2,1)S(1)}, bf16[128,2048]{1,0:T(8,128)(2,1)S(1)}, u32[]{:S(2)}, u32[]{:S(2)}) collective-permute-start(bf16[128,2048]{1,0:T(8,128)(2,1)S(1)} %get-tuple-element.40.near), channel_id=1, source_target_pairs={{0,24},{24,0},{8,16},{16,8},{1,25},{25,1},{9,17},{17,9},{2,26},{26... | collective-permute-start | bytes 1572872 | tf_op jit(solution)/shard_map/ppermute | solution.py:338
  52.3 9.7 %all_to_all.47.got = f32[4,32,128]{2,1,0:T(8,128)S(1)} all-to-all(f32[4,32,128]{2,1,0:T(8,128)S(1)} %shard_map.149), channel_id=1, replica_groups=mesh['z'=16,'y'=4,'tp'=8] {'y'}, dimensions={0} | all-to-all | bytes 131072 | tf_op jit(solution)/shard_map/all_to_all | solution.py:22
  62.0 0.8 shard_map.150
  62.8 9.7 %all-to-all-start.4 = ((bf16[16,24,128]{2,1,0:T(8,128)(2,1)}), bf16[16,24,128]{2,1,0:T(8,128)(2,1)S(1)}, u32[]{:S(2)}, u32[]{:S(2)}) async-start(bf16[16,24,128]{2,1,0:T(8,128)(2,1)} %shard_map.150), calls=%async_computation.4 | async-start | bytes 196608 | tf_op jit(solution)/shard_map/all_to_all | solution.py:22
  72.5 1.9 %collective-permute-start.2 = (bf16[64,2048]{1,0:T(8,128)(2,1)S(1)}, bf16[64,2048]{1,0:T(8,128)(2,1)S(1)}, u32[]{:S(2)}, u32[]{:S(2)}) collective-permute-start(bf16[64,2048]{1,0:T(8,128)(2,1)S(1)} %bitcast.6), channel_id=1, source_target_pairs={{0,8},{8,0},{16,24},{24,16},{1,9},{9,1},{17,25},{25,17},{2,10},{10... | collective-permute-start | bytes 786440 | tf_op jit(solution)/shard_map/ppermute | solution.py:334
  74.4 9.9 %all-to-all-done.4.got = bf16[16,24,128]{2,1,0:T(8,128)(2,1)S(1)} async-done(((bf16[16,24,128]{2,1,0:T(8,128)(2,1)}), bf16[16,24,128]{2,1,0:T(8,128)(2,1)S(1)}, u32[]{:S(2)}, u32[]{:S(2)}) %all-to-all-start.4) | async-done | bytes 98336 | tf_op jit(solution)/shard_map/all_to_all | solution.py:22
  84.3 1.0 shard_map.151
  85.3 11.6 %all-to-all-start.5 = ((f32[8,24,128]{2,1,0:T(8,128)}), f32[8,24,128]{2,1,0:T(8,128)S(1)}, u32[]{:S(2)}, u32[]{:S(2)}) async-start(f32[8,24,128]{2,1,0:T(8,128)} %shard_map.151), calls=%async_computation.5 | async-start | bytes 196608 | tf_op jit(solution)/shard_map/all_to_all | solution.py:22
  96.9 0.0 collective-permute-done.2.other
  96.9 5.0 %all-to-all-done.5.got = f32[8,24,128]{2,1,0:T(8,128)S(1)} async-done(((f32[8,24,128]{2,1,0:T(8,128)}), f32[8,24,128]{2,1,0:T(8,128)S(1)}, u32[]{:S(2)}, u32[]{:S(2)}) %all-to-all-start.5) | async-done | bytes 98336 | tf_op jit(solution)/shard_map/all_to_all | solution.py:22
  101.9 0.0 collective-permute-done.1.far
  101.9 0.4 shard_map.152
  102.3 2.8 %collective-permute-start.3 = (bf16[128,2048]{1,0:T(8,128)(2,1)S(1)}, bf16[128,2048]{1,0:T(8,128)(2,1)S(1)}, u32[]{:S(2)}, u32[]{:S(2)}) collective-permute-start(bf16[128,2048]{1,0:T(8,128)(2,1)S(1)} %get-tuple-element.44.near), channel_id=1, source_target_pairs={{0,24},{24,0},{8,16},{16,8},{1,25},{25,1},{9,17},{17,9},{2,26},{26... | collective-permute-start | bytes 1572872 | tf_op jit(solution)/shard_map/ppermute | solution.py:338
  105.1 14.5 %all_to_all.48.got = bf16[16,16,128]{2,1,0:T(8,128)(2,1)S(1)} all-to-all(bf16[16,16,128]{2,1,0:T(8,128)(2,1)S(1)} %get-tuple-element.42), channel_id=1, replica_groups=mesh['z'=16,'y'=4,'tp'=8] {'z'}, dimensions={0} | all-to-all | bytes 131072 | tf_op jit(solution)/shard_map/all_to_all | solution.py:22
  119.6 0.2 shard_map.153
  119.8 14.3 %all_to_all.49.got = bf16[16,8,128]{2,1,0:T(8,128)(2,1)S(1)} all-to-all(bf16[16,8,128]{2,1,0:T(8,128)(2,1)S(1)} %shard_map.153), channel_id=1, replica_groups=mesh['z'=16,'y'=4,'tp'=8] {'z'}, dimensions={0} | all-to-all | bytes 65536 | tf_op jit(solution)/shard_map/all_to_all | solution.py:22
  134.0 0.0 collective-permute-done.3.far
  134.0 0.4 shard_map.154
  134.5 15.2 %all_to_all.50.got = f32[32,8,128]{2,1,0:T(8,128)S(1)} all-to-all(f32[32,8,128]{2,1,0:T(8,128)S(1)} %shard_map.154), channel_id=1, replica_groups=mesh['z'=16,'y'=4,'tp'=8] {'y','tp'}, dimensions={0} | all-to-all | bytes 262144 | tf_op jit(solution)/shard_map/all_to_all | solution.py:22
  149.7 0.6 shard_map.155
  (3 shorter events, 0.0 us)
Async XLA Ops:
  12.3 26.8 %all-to-all-start.1 = ((bf16[16,24,128]{2,1,0:T(8,128)(2,1)}), bf16[16,24,128]{2,1,0:T(8,128)(2,1)S(1)}, u32[]{:S(2)}, u32[]{:S(2)}) async-start(bf16[16,24,128]{2,1,0:T(8,128)(2,1)} %get-tuple-element.26), calls=%async_computation.1 | async-start | bytes 196608 | tf_op jit(solution)/shard_map/all_to_all | solution.py:22
  27.2 7.6 %collective-permute-start = (bf16[64,2048]{1,0:T(8,128)(2,1)}, bf16[64,2048]{1,0:T(8,128)(2,1)S(1)}, u32[]{:S(2)}, u32[]{:S(2)}) collective-permute-start(bf16[64,2048]{1,0:T(8,128)(2,1)} %w_up.1), channel_id=1, source_target_pairs={{0,8},{8,0},{16,24},{24,16},{1,9},{9,1},{17,25},{25,17},{2,10},{10... | collective-permute-start | bytes 786440 | tf_op jit(solution)/shard_map/ppermute | solution.py:334
  34.8 0.7 copy-start.1
  46.7 25.7 %copy-start = (bf16[2048,64]{0,1:T(8,128)(2,1)S(1)}, bf16[2048,64]{0,1:T(8,128)(2,1)}, u32[]{:S(2)}) copy-start(bf16[2048,64]{0,1:T(8,128)(2,1)} %param.29) | copy-start | bytes 786436
  49.5 52.4 %collective-permute-start.1 = (bf16[128,2048]{1,0:T(8,128)(2,1)S(1)}, bf16[128,2048]{1,0:T(8,128)(2,1)S(1)}, u32[]{:S(2)}, u32[]{:S(2)}) collective-permute-start(bf16[128,2048]{1,0:T(8,128)(2,1)S(1)} %get-tuple-element.40.near), channel_id=1, source_target_pairs={{0,24},{24,0},{8,16},{16,8},{1,25},{25,1},{9,17},{17,9},{2,26},{26... | collective-permute-start | bytes 1572872 | tf_op jit(solution)/shard_map/ppermute | solution.py:338
  62.8 21.5 %all-to-all-start.4 = ((bf16[16,24,128]{2,1,0:T(8,128)(2,1)}), bf16[16,24,128]{2,1,0:T(8,128)(2,1)S(1)}, u32[]{:S(2)}, u32[]{:S(2)}) async-start(bf16[16,24,128]{2,1,0:T(8,128)(2,1)} %shard_map.150), calls=%async_computation.4 | async-start | bytes 196608 | tf_op jit(solution)/shard_map/all_to_all | solution.py:22
  72.5 24.4 %collective-permute-start.2 = (bf16[64,2048]{1,0:T(8,128)(2,1)S(1)}, bf16[64,2048]{1,0:T(8,128)(2,1)S(1)}, u32[]{:S(2)}, u32[]{:S(2)}) collective-permute-start(bf16[64,2048]{1,0:T(8,128)(2,1)S(1)} %bitcast.6), channel_id=1, source_target_pairs={{0,8},{8,0},{16,24},{24,16},{1,9},{9,1},{17,25},{25,17},{2,10},{10... | collective-permute-start | bytes 786440 | tf_op jit(solution)/shard_map/ppermute | solution.py:334
  85.3 16.6 %all-to-all-start.5 = ((f32[8,24,128]{2,1,0:T(8,128)}), f32[8,24,128]{2,1,0:T(8,128)S(1)}, u32[]{:S(2)}, u32[]{:S(2)}) async-start(f32[8,24,128]{2,1,0:T(8,128)} %shard_map.151), calls=%async_computation.5 | async-start | bytes 196608 | tf_op jit(solution)/shard_map/all_to_all | solution.py:22
  102.3 31.8 %collective-permute-start.3 = (bf16[128,2048]{1,0:T(8,128)(2,1)S(1)}, bf16[128,2048]{1,0:T(8,128)(2,1)S(1)}, u32[]{:S(2)}, u32[]{:S(2)}) collective-permute-start(bf16[128,2048]{1,0:T(8,128)(2,1)S(1)} %get-tuple-element.44.near), channel_id=1, source_target_pairs={{0,24},{24,0},{8,16},{16,8},{1,25},{25,1},{9,17},{17,9},{2,26},{26... | collective-permute-start | bytes 1572872 | tf_op jit(solution)/shard_map/ppermute | solution.py:338
